TPU v7x, 32 devices: a whole 2x2x4 slice. The times are simulated.
32 devices in a mesh: ep: 16 (over z, x, core), tp: 2 (over y).
Axes of the slice: x: 2, y: 2, z: 4, core: 2. Of those that a mesh axis runs over, the one named last changes fastest.
Arguments:
- residual_in: bfloat16 [240, 1536], P('ep'), may hold values from -6 to 6
- rec_state: bfloat16 [240, 12, 128, 128], P('ep', 'tp'), may hold values from -6 to 6
- mix_gain: float32 [1536], replicated, may hold values from 0.1 to 1.9
- w_query: bfloat16 [1536, 1536], P('tp', 'ep'), may hold values from -0.15625 to 0.15625
- w_forget: bfloat16 [1536, 1536], P('tp', 'ep'), may hold values from -0.15625 to 0.15625
- w_input: bfloat16 [1536, 1536], P('tp', 'ep'), may hold values from -0.15625 to 0.15625
- w_gate: bfloat16 [1536, 1536], P('tp', 'ep'), may hold values from -0.15625 to 0.15625
- lower_bound: float32 [1536], P('tp'), may hold values from 0 to 0.9
- head_gain: float32 [128], replicated, may hold values from 0.1 to 1.9
- w_out: bfloat16 [1536, 1536], P('tp', 'ep'), may hold values from -0.15625 to 0.15625
- ffn_gain: float32 [1536], replicated, may hold values from 0.1 to 1.9
- route_ids: int32 [240, 6], P('ep'), may hold values from 0 to 15, all different within a row; in each aligned block of 15 rows (0 to 14, 15 to 29, ...) at most 6 rows name the same one
- route_weight: float32 [240, 6], P('ep'), may hold values from 0.2 to 1
- expert_gate: bfloat16 [16, 1536, 512], P('ep', None, 'tp'), may hold values from -0.15625 to 0.15625
- expert_up: bfloat16 [16, 1536, 512], P('ep', None, 'tp'), may hold values from -0.15625 to 0.15625
- expert_down: bfloat16 [16, 512, 1536], P('ep', 'tp'), may hold values from -0.25 to 0.25
Outputs:
- layer_out: bfloat16 [240, 1536], P('ep', 'tp')
- new_state: bfloat16 [240, 12, 128, 128], P('ep', 'tp')
Inputs may be any that keep to these rules, and one draw needn't show every extreme that they name: `route_ids`: each row names 6 different experts. Among the rows of one device no expert is named more than 6 times, and in every draw some device names some expert exactly 6 times.
All inputs are finite; a program needn't handle non-finite values.
Results may differ from a plain program's by a relative error of at most 0.016.
Values may be sent and summed in bfloat16 or wider, within the bound.
No kernel may reach another device: no remote copies, remote signals or barrier semaphores. Data moves between devices by JAX's collectives and lax.ppermute only.
A program may use at most 64 MiB of HBM per device.

v0:
```python
import functools

import jax
import jax.numpy as jnp
from jax import lax
from jax.experimental import pallas as pl
from jax.experimental.pallas import tpu as pltpu
from jax.sharding import Mesh, PartitionSpec as P


rms_eps = 1e-06
bf16, f32 = jnp.bfloat16, jnp.float32


def dot(a, b):
    return jnp.dot(a, b, preferred_element_type=f32)


def rms_scale(values, gain):
    return values * lax.rsqrt(jnp.mean(values * values, axis=-1, keepdims=True) + rms_eps) * gain


def up(n, m):
    return -(-n // m) * m


def call(body, out_shape, *args, mib=16, cost=None, **kw):
    return pl.pallas_call(
        body,
        out_shape=out_shape,
        compiler_params=pltpu.CompilerParams(vmem_limit_bytes=mib << 20),
        cost_estimate=cost,
        **kw,
    )(*args)


def dot_t(a, b):
    return lax.dot_general(a, b, (((1,), (1,)), ((), ())), preferred_element_type=f32)


def pick_part(rank, full, part):
    own = full[:, :part]
    for t in range(1, full.shape[1] // part):
        own = jnp.where(rank == t, full[:, t * part : (t + 1) * part], own)
    return own


def core_order(core, own, other):
    return jnp.where(core == 0, own, other), jnp.where(core == 0, other, own)


def norm_body(*refs):
    sources, (out_ref, own_ref, mix_ref, res_ref, gain_ref, sems) = refs[:7], refs[7:]
    targets = [res_ref, gain_ref] + [own_ref.at[p] for p in range(4)] + [mix_ref]
    loads = [
        pltpu.make_async_copy(source, target, sems.at[i])
        for i, (source, target) in enumerate(zip(sources, targets))
    ]
    for load in loads:
        load.start()
    groups, rows, part = out_ref.shape
    tp_rank = lax.axis_index("tp")
    for load in loads[:2]:
        load.wait()
    res = res_ref[...].astype(f32)
    scale = lax.rsqrt(jnp.mean(res * res, axis=-1, keepdims=True) + rms_eps)
    normed = (res * scale * gain_ref[...].reshape(1, -1)).astype(bf16)
    half = pick_part(tp_rank, normed, part)
    half = jnp.concatenate([half, jnp.zeros((rows - half.shape[0], part), bf16)], axis=0)
    for g in range(groups):
        out_ref[g] = half
    for load in loads[2:]:
        load.wait()


def proj_body(x_ref, own_ref, oth_ref, out_ref):
    groups, rows, part = x_ref.shape
    half = out_ref.shape[-1] // 2
    x = x_ref[...].reshape(groups * rows, part)
    for i, w_ref in enumerate((own_ref, oth_ref)):
        columns = jnp.concatenate([w_ref[p] for p in range(4)], axis=0)
        y = dot_t(x, columns).astype(bf16).reshape(groups, rows, half)
        for t in range(out_ref.shape[1]):
            out_ref[:, t, :, i * half : (i + 1) * half] = y


def pack_body(own_ref, far_ref, out_ref):
    high = lax.axis_index("a") // 2
    out_ref[high] = own_ref[...]
    out_ref[1 - high] = far_ref[...]


def read_body(recv_ref, lower_ref, gain_ref, state_ref, out_ref, forget_ref, value_ref):
    groups, tp_count, rows, both = recv_ref.shape
    seqs, heads, size, _ = state_ref.shape
    pieces = groups // tp_count
    first = lax.axis_index("tp") * pieces
    core = lax.axis_index("c")
    blocks = [recv_ref[first + g].astype(f32).sum(axis=0) for g in range(pieces)]
    cols = both // 8
    proj = []
    for p in range(4):
        parts = []
        for block in blocks:
            own = block[:, p * cols : (p + 1) * cols]
            other = block[:, both // 2 + p * cols : both // 2 + (p + 1) * cols]
            parts += core_order(core, own, other)
        proj.append(jnp.concatenate(parts, axis=1).astype(bf16).astype(f32))
    query = jax.nn.silu(proj[0])
    lower = lower_ref[...].reshape(1, -1)
    forget = lower + (1.0 - lower) * jax.nn.sigmoid(proj[1])
    forget_ref[...] = forget
    value_ref[...] = proj[2]
    gate = jax.nn.silu(proj[3])
    gain = gain_ref[...].reshape(1, -1)
    mixed = query * forget
    high = mixed.astype(bf16)
    low = (mixed - high.astype(f32)).astype(bf16)
    direct = query * (1.0 - forget)
    row_ids = lax.broadcasted_iota(jnp.int32, (rows, size), 0)
    for h in range(heads):
        lanes = slice(h * size, (h + 1) * size)
        lhs = jnp.concatenate([high[:, lanes], low[:, lanes]], axis=0)
        readout = jnp.sum(direct[:, lanes], axis=1, keepdims=True) * proj[2][:, lanes]
        for s in range(seqs):
            both_parts = dot(lhs, state_ref[s, h])
            readout += jnp.where(row_ids == s, both_parts[:rows] + both_parts[rows:], 0.0)
        heads_out = (rms_scale(readout, gain) * gate[:, lanes]).astype(bf16)
        for g in range(out_ref.shape[0]):
            out_ref[g, :, lanes] = heads_out


def state_body(forget_ref, value_ref, state_ref, new_ref):
    seqs = state_ref.shape[0]
    forget_t = forget_ref[...].T
    key_t = 1.0 - forget_t
    value = value_ref[...]
    for s in range(seqs):
        new_ref[s, 0] = (
            forget_t[:, s : s + 1] * state_ref[s, 0].astype(f32)
            + key_t[:, s : s + 1] * value[s : s + 1]
        ).astype(bf16)


def mix_body(x_ref, *refs):
    *w_refs, out_ref = refs
    blocks, rows, part = x_ref.shape
    x = x_ref[...].reshape(blocks * rows, part)
    ys = [dot_t(x, w_ref[...].reshape(-1, part)) for w_ref in w_refs]
    if len(ys) == 2:
        cols = ys[0].shape[1] // 2
        low = lax.rem(lax.axis_index("a"), 2)
        ys = [
            y
            for high in range(2)
            for y in core_order(low, *(y[:, high * cols : (high + 1) * cols] for y in ys))
        ]
    y = jnp.concatenate(ys, axis=1).astype(bf16).reshape(blocks, rows, -1)
    for t in range(out_ref.shape[1]):
        out_ref[:, t] = y


def slots_of(ids, slots, experts):
    tops, seqs = ids.shape
    row = lax.broadcasted_iota(jnp.int32, (experts * slots, seqs), 0)
    expert, place = row // slots, row % slots
    named = [ids[k : k + 1] == expert for k in range(tops)]
    names = sum(n.astype(f32) for n in named)
    before = (
        lax.broadcasted_iota(jnp.int32, (seqs, seqs), 0)
        < lax.broadcasted_iota(jnp.int32, (seqs, seqs), 1)
    ).astype(f32)
    rank = dot(names.astype(bf16), before.astype(bf16))
    here = jnp.where(rank == place.astype(f32), names, 0.0)
    return here, named


def dispatch_body(recv_ref, res_ref, gain_ref, ids_ref, out_ref, own_ref, lines):
    blocks = recv_ref.shape[0]
    deep = lax.axis_size("a")
    cols = recv_ref.shape[3] // deep
    seqs, width = res_ref.shape
    per_row = width // 128
    slots_all = out_ref.shape[0] // per_row
    experts = deep * blocks
    sums = [recv_ref[g].astype(f32).sum(axis=0) for g in range(blocks)]
    mixed = jnp.concatenate(
        [x[:, a * cols : (a + 1) * cols] for a in range(deep) for x in sums], axis=1
    )[:seqs]
    after = (res_ref[...].astype(f32) + mixed).astype(bf16).astype(f32)
    normed = rms_scale(after, gain_ref[...].reshape(1, -1)).astype(bf16)
    here, _ = slots_of(ids_ref[...], slots_all // experts, experts)
    picked = dot(here.astype(bf16), normed)
    for j in range(per_row):
        lines[pl.ds(j, slots_all, stride=per_row), :] = picked[:, j * 128 : (j + 1) * 128]
    out_ref[...] = lines[...].astype(bf16)
    own_ref[...] = pick_part(lax.axis_index("tp"), after, own_ref.shape[1])


def expert_body(capacity, x_ref, gate_ref, up_ref, down_ref, out_ref, lines, sent):
    width = gate_ref.shape[1]
    per_row = width // 128
    count = x_ref.shape[0]
    sources = count // (capacity * per_row)
    lines[:count] = x_ref[...].astype(f32)
    lines[count:] = jnp.zeros((lines.shape[0] - count, 128), f32)
    x = jnp.concatenate(
        [
            jnp.concatenate(
                [
                    lines[pl.ds(e * capacity * per_row + j, 8, stride=per_row), :]
                    for j in range(per_row)
                ],
                axis=1,
            )
            for e in range(sources)
        ],
        axis=0,
    ).astype(bf16)
    hidden = (jax.nn.silu(dot(x, gate_ref[0])) * dot(x, up_ref[0])).astype(bf16)
    y = dot(hidden, down_ref[0])
    targets, chunk, _ = out_ref.shape
    tp_count = targets // sources
    per_part = per_row // tp_count
    for d in range(targets):
        e, t = d // tp_count, d % tp_count
        for j in range(per_part):
            lane = (t * per_part + j) * 128
            sent[pl.ds(d * chunk + j, 8, stride=per_part), :] = y[
                e * 8 : (e + 1) * 8, lane : lane + 128
            ]
    for d in range(targets):
        out_ref[d] = sent[d * chunk : (d + 1) * chunk].astype(bf16)


def combine_body(back_ref, ids_ref, weight_ref, own_ref, out_ref, lines):
    targets, chunk, _ = back_ref.shape
    tp_count = lax.axis_size("tp")
    experts = targets // tp_count
    per_part = own_ref.shape[1] // 128
    for d in range(targets):
        lines[d * chunk : (d + 1) * chunk] = back_ref[d].astype(f32)
    lines[targets * chunk :] = jnp.zeros((lines.shape[0] - targets * chunk, 128), f32)

    def piece(e, j):
        return sum(
            lines[pl.ds((e * tp_count + t) * chunk + j, 8, stride=per_part), :]
            for t in range(tp_count)
        )

    rows = jnp.concatenate(
        [
            jnp.concatenate([piece(e, j) for j in range(per_part)], axis=1)
            for e in range(experts)
        ],
        axis=0,
    ).astype(bf16)
    here, named = slots_of(ids_ref[...], 8, experts)
    weight = sum(jnp.where(n, weight_ref[k : k + 1], 0.0) for k, n in enumerate(named))
    weight = weight * here
    high = weight.astype(bf16)
    low = (weight - high.astype(f32)).astype(bf16)
    total = sum(
        lax.dot_general(w, rows, (((0,), (0,)), ((), ())), preferred_element_type=f32)
        for w in (high, low)
    )
    out_ref[...] = (own_ref[...] + total).astype(bf16)


def capacity_of(seqs, tops, experts):
    return max(2, seqs * tops // experts + 1)


def shards(
    residual_in,
    rec_state,
    mix_gain,
    w_query,
    w_forget,
    w_input,
    w_gate,
    lower_bound,
    head_gain,
    w_out,
    ffn_gain,
    route_ids,
    route_weight,
    expert_gate,
    expert_up,
    expert_down,
):
    deep, wide, cores, tp_count = (lax.axis_size(a) for a in ("a", "b", "c", "tp"))
    groups, plane = deep * wide, wide * cores
    chips = ("a", "b")
    seqs, width = residual_in.shape
    part = width // tp_count
    cols = w_query.shape[1]
    _, heads, size, _ = rec_state.shape
    rows = up(seqs, 16)
    sds = jax.ShapeDtypeStruct

    sources = [residual_in, mix_gain]
    sources += [w.T for w in (w_query, w_forget, w_input, w_gate, w_out)]
    vmem, hbm = (pl.BlockSpec(memory_space=m) for m in (pltpu.VMEM, pltpu.HBM))
    spread, own_w, own_o = call(
        norm_body,
        [
            sds((groups, rows, part), bf16),
            sds((4, cols, part), bf16),
            sds((cols, part), bf16),
        ],
        *(pltpu.with_memory_space_constraint(a, pltpu.HBM) for a in sources),
        in_specs=[hbm] * 7,
        out_specs=[vmem] * 3,
        scratch_shapes=[
            pltpu.VMEM(residual_in.shape, bf16),
            pltpu.VMEM(mix_gain.shape, f32),
            pltpu.SemaphoreType.DMA((7,)),
        ],
    )
    oth_w = lax.ppermute(own_w, "c", [(i, i ^ 1) for i in range(cores)])
    if deep == 4:
        far = lax.ppermute(own_o, "a", [(i, i ^ 2) for i in range(deep)])
    gathered = lax.all_to_all(spread, chips, 0, 0, tiled=True)

    partial = call(
        proj_body,
        sds((groups, tp_count, rows, 4 * cores * cols), bf16),
        gathered,
        own_w,
        oth_w,
    )
    if deep == 4:
        packs = [call(pack_body, sds((2, cols, part), bf16), own_o, far)]
        packs.append(lax.ppermute(packs[0], "a", [(i, i ^ 1) for i in range(deep)]))
    else:
        packs = [lax.all_gather(own_o, "a", axis=0).reshape(deep * cols, part)]
    arrived = lax.all_to_all(
        partial.reshape(groups * tp_count, rows, -1), (*chips, "tp"), 0, 0, tiled=True
    ).reshape(partial.shape)

    spread_heads, forget, value = call(
        read_body,
        [
            sds((plane, rows, heads * size), bf16),
            sds((rows, heads * size), f32),
            sds((rows, heads * size), f32),
        ],
        arrived,
        lower_bound,
        head_gain,
        rec_state,
    )
    if deep == 4:
        spread_heads, packs[1] = lax.optimization_barrier((spread_heads, packs[1]))
    all_heads = lax.all_to_all(spread_heads, ("b", "c"), 0, 0, tiled=True)

    per_head = pl.BlockSpec((seqs, 1, size, size), lambda i: (0, i, 0, 0))
    head_lanes = pl.BlockSpec((rows, size), lambda i: (0, i))
    new_state = call(
        state_body,
        sds(rec_state.shape, bf16),
        forget,
        value,
        rec_state,
        grid=(heads,),
        in_specs=[head_lanes, head_lanes, per_head],
        out_specs=per_head,
        cost=pl.CostEstimate(
            flops=10**7, bytes_accessed=4 * rec_state.size, transcendentals=0
        ),
    )

    partial_mix = call(
        mix_body, sds((plane, tp_count, rows, deep * cols), bf16), all_heads, *packs
    )
    mix_home = lax.all_to_all(
        partial_mix.reshape(plane * tp_count, rows, -1), ("b", "c", "tp"), 0, 0, tiled=True
    ).reshape(partial_mix.shape)

    experts = groups * cores
    capacity = capacity_of(seqs, route_ids.shape[1], experts)
    assert capacity <= 8
    lines = experts * capacity * width // 128
    buffer, own_mix = call(
        dispatch_body,
        [sds((lines, 128), bf16), sds((seqs, part), f32)],
        mix_home,
        residual_in,
        ffn_gain,
        route_ids.T,
        scratch_shapes=[pltpu.VMEM((lines, 128), f32)],
    )
    received = lax.all_to_all(
        buffer.reshape(experts, -1, 128), (*chips, "c"), 0, 0, tiled=True
    ).reshape(lines, 128)
    per_part = part // 128
    chunk = up(capacity * per_part, 8)
    targets = experts * tp_count
    sent = targets * chunk + 8 * per_part
    down = call(
        functools.partial(expert_body, capacity),
        sds((targets, chunk, 128), bf16),
        received,
        expert_gate,
        expert_up,
        expert_down,
        scratch_shapes=[
            pltpu.VMEM((lines + 8 * width // 128, 128), f32),
            pltpu.VMEM((sent, 128), f32),
        ],
    )
    back = lax.all_to_all(down, (*chips, "c", "tp"), 0, 0, tiled=True)
    layer_out = call(
        combine_body,
        sds((seqs, part), bf16),
        back,
        route_ids.T,
        route_weight.T,
        own_mix,
        scratch_shapes=[pltpu.VMEM((sent, 128), f32)],
    )
    return layer_out, new_state


def solution(mesh):
    ep, tp = mesh.shape["ep"], mesh.shape["tp"]
    wide = 2 if ep % 4 == 0 else 1
    shape = (ep // (2 * wide), wide, 2, tp)
    split = Mesh(mesh.devices.reshape(shape), ("a", "b", "c", "tp"))
    seq = ("a", "b", "c")
    in_specs = (
        P(seq, None),
        P(seq, "tp", None, None),
        P(),
        P("tp", seq),
        P("tp", seq),
        P("tp", seq),
        P("tp", seq),
        P("tp"),
        P(),
        P("tp", seq),
        P(),
        P(seq, None),
        P(seq, None),
        P(seq, None, "tp"),
        P(seq, None, "tp"),
        P(seq, "tp", None),
    )
    out_specs = (P(seq, "tp"), P(seq, "tp", None, None))
    return jax.shard_map(
        shards, mesh=split, in_specs=in_specs, out_specs=out_specs, check_vma=False
    )
```

profile of v0, /device:TPU:0, one launch (start us, length us, event | category | flops | bytes accessed | tf_op | source)
XLA Modules:
  0.0 97.1 jit_solution(16743131920336776997)
XLA Ops:
  0.6 0.0 copy-start
  0.6 0.0 copy-start.7
  0.7 1.4 %shard_map.167 = (bf16[8,16,768]{2,1,0:T(8,128)(2,1)S(1)}, bf16[4,96,768]{2,1,0:T(8,128)(2,1)S(1)}, bf16[96,768]{1,0:T(8,128)(2,1)S(1)}) custom-call(bf16[15,1536]{1,0:T(8,128)(2,1)} %res_ref.1, f32[1536]{0:T(1024)} %refs_1_.1, bf16[96,768]{1,0:T(8,128)(2,1)} %bitcast.21, bf16[96,768]{1,0:T(8,128)(2,1)} %bitcast.22, bf16[96,768]{1,0:T(8,128)(2,1)} %bitcast.23, ...), custom_call_target="tpu_custom_call" | custom-call | tf_op jit(solution)/shard_map/pallas_call | solution.py:28
  2.1 0.6 collective-permute-start
  2.7 15.2 %all_to_all.30.x_ref = bf16[8,16,768]{2,1,0:T(8,128)(2,1)S(1)} all-to-all(bf16[8,16,768]{2,1,0:T(8,128)(2,1)S(1)} %get-tuple-element.12), channel_id=1, replica_groups=mesh['a'=4,'b'=2,'c'=2,'tp'=2] {'a','b'}, dimensions={0} | all-to-all | bytes 393216 | tf_op jit(solution)/shard_map/all_to_all | solution.py:324
  17.9 0.0 collective-permute-done.oth_ref
  17.9 1.2 %shard_map.168 = bf16[8,2,16,768]{3,2,1,0:T(8,128)(2,1)} custom-call(bf16[8,16,768]{2,1,0:T(8,128)(2,1)S(1)} %all_to_all.30.x_ref, bf16[4,96,768]{2,1,0:T(8,128)(2,1)S(1)} %get-tuple-element.13.own_ref, bf16[4,96,768]{2,1,0:T(8,128)(2,1)S(1)} %collective-permute-done.oth_ref), custom_call_target="tpu_custom_call" | custom-call | tf_op jit(solution)/shard_map/pallas_call | solution.py:28
  19.1 0.0 copy-start.4
  19.1 0.0 copy-start.5
  19.1 0.0 copy-start.6
  19.1 4.3 %all-to-all-start.1 = ((bf16[16,16,768]{2,1,0:T(8,128)(2,1)}), bf16[16,16,768]{2,1,0:T(8,128)(2,1)S(1)}, u32[]{:S(2)}, u32[]{:S(2)}) async-start(bf16[16,16,768]{2,1,0:T(8,128)(2,1)} %bitcast.5), calls=%async_computation.1 | async-start | bytes 786432 | tf_op jit(solution)/shard_map/all_to_all | solution.py:338
  23.4 2.8 %collective-permute-start.1 = (bf16[96,768]{1,0:T(8,128)(2,1)S(1)}, bf16[96,768]{1,0:T(8,128)(2,1)S(1)}, u32[]{:S(2)}, u32[]{:S(2)}) collective-permute-start(bf16[96,768]{1,0:T(8,128)(2,1)S(1)} %get-tuple-element.15.own_ref), channel_id=1, source_target_pairs={{0,16},{8,24},{16,0},{24,8},{1,17},{9,25},{17,1},{25,9},{2,18},{10... | collective-permute-start | bytes 442376 | tf_op jit(solution)/shard_map/ppermute | solution.py:323
  26.3 15.2 %collective-permute-done.1.far_ref = bf16[96,768]{1,0:T(8,128)(2,1)S(1)} collective-permute-done((bf16[96,768]{1,0:T(8,128)(2,1)S(1)}, bf16[96,768]{1,0:T(8,128)(2,1)S(1)}, u32[]{:S(2)}, u32[]{:S(2)}) %collective-permute-start.1) | collective-permute-done | bytes 147488 | tf_op jit(solution)/shard_map/ppermute | solution.py:323
  41.4 0.7 shard_map.170.refs_0_
  42.2 0.0 collective-permute-start.2
  42.2 0.0 all-to-all-done.1
  42.2 0.0 copy-start.1
  42.2 0.0 copy-start.2
  42.2 0.0 copy-start.3
  42.2 0.0 copy-done
  42.2 0.0 copy-done.7
  42.2 0.0 copy-start.9
  42.2 0.8 copy-done.9
  43.0 1.1 %shard_map.169 = (bf16[4,16,768]{2,1,0:T(8,128)(2,1)S(1)}, f32[16,768]{1,0:T(8,128)S(1)}, f32[16,768]{1,0:T(8,128)S(1)}) custom-call(bf16[8,2,16,768]{3,2,1,0:T(8,128)(2,1)S(1)} %bitcast.13, f32[768]{0:T(1024)S(1)} %copy-done.7, f32[128]{0:T(128)S(1)} %copy-done.9, bf16[15,6,128,128]{3,2,1,0:T(8,128)(2,1)S(1)} %copy-done), custom_call_target="tpu_custom_call" | custom-call | tf_op jit(solution)/shard_map/pallas_call | solution.py:28
  44.1 6.4 %collective-permute-done.2.refs_1_ = bf16[2,96,768]{2,1,0:T(8,128)(2,1)} collective-permute-done((bf16[2,96,768]{2,1,0:T(8,128)(2,1)}, bf16[2,96,768]{2,1,0:T(8,128)(2,1)}, u32[]{:S(2)}, u32[]{:S(2)}) %collective-permute-start.2) | collective-permute-done | bytes 294944 | tf_op jit(solution)/shard_map/ppermute | solution.py:335
  50.5 6.8 %all_to_all.31.x_ref = bf16[4,16,768]{2,1,0:T(8,128)(2,1)S(1)} all-to-all(bf16[4,16,768]{2,1,0:T(8,128)(2,1)S(1)} %get-tuple-element.16), channel_id=1, replica_groups=mesh['a'=4,'b'=2,'c'=2,'tp'=2] {'b','c'}, dimensions={0} | all-to-all | bytes 196608 | tf_op jit(solution)/shard_map/all_to_all | solution.py:356
  57.3 1.4 %shard_map.171 = bf16[4,2,16,384]{3,2,1,0:T(8,128)(2,1)S(1)} custom-call(bf16[4,16,768]{2,1,0:T(8,128)(2,1)S(1)} %all_to_all.31.x_ref, bf16[2,96,768]{2,1,0:T(8,128)(2,1)} %shard_map.170.refs_0_, bf16[2,96,768]{2,1,0:T(8,128)(2,1)} %collective-permute-done.2.refs_1_), custom_call_target="tpu_custom_call" | custom-call | tf_op jit(solution)/shard_map/pallas_call | solution.py:28
  58.7 7.3 %all_to_all.32 = bf16[8,16,384]{2,1,0:T(8,128)(2,1)S(1)} all-to-all(bf16[8,16,384]{2,1,0:T(8,128)(2,1)S(1)} %bitcast.15), channel_id=1, replica_groups=mesh['a'=4,'b'=2,'c'=2,'tp'=2] {'b','c','tp'}, dimensions={0} | all-to-all | bytes 196608 | tf_op jit(solution)/shard_map/all_to_all | solution.py:377
  66.0 0.0 copy-done.4
  66.0 0.0 copy-done.5
  66.1 0.0 copy-done.6
  66.1 0.4 shard_map.172
  66.5 14.0 %all_to_all.33 = bf16[16,72,128]{2,1,0:T(8,128)(2,1)S(1)} all-to-all(bf16[16,72,128]{2,1,0:T(8,128)(2,1)S(1)} %bitcast.17), channel_id=1, replica_groups=mesh['a'=4,'b'=2,'c'=2,'tp'=2] {'a','b','c'}, dimensions={0} | all-to-all | bytes 589824 | tf_op jit(solution)/shard_map/all_to_all | solution.py:394
  80.4 0.0 copy-done.1
  80.4 0.0 copy-done.2
  80.4 0.0 copy-done.3
  80.5 1.4 %shard_map.173 = bf16[32,40,128]{2,1,0:T(8,128)(2,1)} custom-call(bf16[1152,128]{1,0:T(8,128)(2,1)S(1)} %bitcast.14, bf16[1,1536,256]{2,1,0:T(8,128)(2,1)S(1)} %copy-done.1, bf16[1,1536,256]{2,1,0:T(8,128)(2,1)S(1)} %copy-done.2, bf16[1,256,1536]{2,1,0:T(8,128)(2,1)S(1)} %copy-done.3), custom_call_target="tpu_custom_call" | custom-call | tf_op jit(solution)/shard_map/pallas_call | solution.py:28
  81.9 2.6 %all-to-all-start.5 = ((bf16[32,40,128]{2,1,0:T(8,128)(2,1)}), bf16[32,40,128]{2,1,0:T(8,128)(2,1)S(1)}, u32[]{:S(2)}, u32[]{:S(2)}) async-start(bf16[32,40,128]{2,1,0:T(8,128)(2,1)} %shard_map.173), calls=%async_computation.5 | async-start | bytes 655360 | tf_op jit(solution)/shard_map/all_to_all | solution.py:413
  84.5 0.0 copy-start.8
  84.5 5.3 %shard_map.175 = bf16[15,6,128,128]{3,2,1,0:T(8,128)(2,1)} custom-call(f32[16,768]{1,0:T(8,128)S(1)} %get-tuple-element.20.forget_ref, f32[16,768]{1,0:T(8,128)S(1)} %get-tuple-element.21.value_ref, bf16[15,6,128,128]{3,2,1,0:T(8,128)(2,1)S(1)} %copy-done), custom_call_target="tpu_custom_call" | custom-call | flops 10000000 | bytes 5898240 | tf_op jit(solution)/shard_map/pallas_call | solution.py:28
  89.8 6.4 %all-to-all-done.5.back_ref = bf16[32,40,128]{2,1,0:T(8,128)(2,1)S(1)} async-done(((bf16[32,40,128]{2,1,0:T(8,128)(2,1)}), bf16[32,40,128]{2,1,0:T(8,128)(2,1)S(1)}, u32[]{:S(2)}, u32[]{:S(2)}) %all-to-all-start.5) | async-done | bytes 327712 | tf_op jit(solution)/shard_map/all_to_all | solution.py:413
  96.2 0.0 copy-done.8
  96.2 1.0 %shard_map.174 = bf16[15,768]{1,0:T(8,128)(2,1)} custom-call(bf16[32,40,128]{2,1,0:T(8,128)(2,1)S(1)} %all-to-all-done.5.back_ref, s32[6,15]{1,0:T(8,128)S(1)} %bitcast.19, f32[6,15]{1,0:T(8,128)S(1)} %bitcast.20, f32[15,768]{1,0:T(8,128)S(1)} %get-tuple-element.19.own_ref), custom_call_target="tpu_custom_call" | custom-call | tf_op jit(solution)/shard_map/pallas_call | solution.py:28
Async XLA Ops:
  0.6 41.6 %copy-start = (bf16[15,6,128,128]{3,2,1,0:T(8,128)(2,1)S(1)}, bf16[15,6,128,128]{3,2,1,0:T(8,128)(2,1)}, u32[]{:S(2)}) copy-start(bf16[15,6,128,128]{3,2,1,0:T(8,128)(2,1)} %state_ref.3) | copy-start | bytes 8847364
  0.6 41.6 %copy-start.7 = (f32[768]{0:T(1024)S(1)}, f32[768]{0:T(1024)}, u32[]{:S(2)}) copy-start(f32[768]{0:T(1024)} %lower_ref.1) | copy-start | bytes 9220
  2.1 15.8 %collective-permute-start = (bf16[4,96,768]{2,1,0:T(8,128)(2,1)S(1)}, bf16[4,96,768]{2,1,0:T(8,128)(2,1)S(1)}, u32[]{:S(2)}, u32[]{:S(2)}) collective-permute-start(bf16[4,96,768]{2,1,0:T(8,128)(2,1)S(1)} %get-tuple-element.13.own_ref), channel_id=1, source_target_pairs={{0,2},{2,0},{1,3},{3,1},{4,6},{6,4},{5,7},{7,5},{8,10},{10,8},{9,1... | collective-permute-start | bytes 1769480 | tf_op jit(solution)/shard_map/ppermute | solution.py:321
  19.1 47.0 %copy-start.4 = (bf16[15,1536]{1,0:T(8,128)(2,1)S(1)}, bf16[15,1536]{1,0:T(8,128)(2,1)}, u32[]{:S(2)}) copy-start(bf16[15,1536]{1,0:T(8,128)(2,1)} %res_ref.1) | copy-start | bytes 138244
  19.1 47.0 %copy-start.5 = (s32[15,6]{0,1:T(8,128)S(1)}, s32[15,6]{0,1:T(8,128)}, u32[]{:S(2)}) copy-start(s32[15,6]{0,1:T(8,128)} %param.27) | copy-start | bytes 1084
  19.1 47.0 %copy-start.6 = (f32[1536]{0:T(1024)S(1)}, f32[1536]{0:T(1024)}, u32[]{:S(2)}) copy-start(f32[1536]{0:T(1024)} %gain_ref.3) | copy-start | bytes 18436
  19.1 23.1 %all-to-all-start.1 = ((bf16[16,16,768]{2,1,0:T(8,128)(2,1)}), bf16[16,16,768]{2,1,0:T(8,128)(2,1)S(1)}, u32[]{:S(2)}, u32[]{:S(2)}) async-start(bf16[16,16,768]{2,1,0:T(8,128)(2,1)} %bitcast.5), calls=%async_computation.1 | async-start | bytes 786432 | tf_op jit(solution)/shard_map/all_to_all | solution.py:338
  23.4 18.0 %collective-permute-start.1 = (bf16[96,768]{1,0:T(8,128)(2,1)S(1)}, bf16[96,768]{1,0:T(8,128)(2,1)S(1)}, u32[]{:S(2)}, u32[]{:S(2)}) collective-permute-start(bf16[96,768]{1,0:T(8,128)(2,1)S(1)} %get-tuple-element.15.own_ref), channel_id=1, source_target_pairs={{0,16},{8,24},{16,0},{24,8},{1,17},{9,25},{17,1},{25,9},{2,18},{10... | collective-permute-start | bytes 442376 | tf_op jit(solution)/shard_map/ppermute | solution.py:323
  42.2 8.3 %collective-permute-start.2 = (bf16[2,96,768]{2,1,0:T(8,128)(2,1)}, bf16[2,96,768]{2,1,0:T(8,128)(2,1)}, u32[]{:S(2)}, u32[]{:S(2)}) collective-permute-start(bf16[2,96,768]{2,1,0:T(8,128)(2,1)} %shard_map.170.refs_0_), channel_id=1, source_target_pairs={{0,8},{8,0},{16,24},{24,16},{1,9},{9,1},{17,25},{25,17},{2,10},{10... | collective-permute-start | bytes 884744 | tf_op jit(solution)/shard_map/ppermute | solution.py:335
  42.2 38.3 %copy-start.1 = (bf16[1,1536,256]{2,1,0:T(8,128)(2,1)S(1)}, bf16[1,1536,256]{2,1,0:T(8,128)(2,1)}, u32[]{:S(2)}) copy-start(bf16[1,1536,256]{2,1,0:T(8,128)(2,1)} %gate_ref.1) | copy-start | bytes 2359300
  42.2 38.3 %copy-start.2 = (bf16[1,1536,256]{2,1,0:T(8,128)(2,1)S(1)}, bf16[1,1536,256]{2,1,0:T(8,128)(2,1)}, u32[]{:S(2)}) copy-start(bf16[1,1536,256]{2,1,0:T(8,128)(2,1)} %up_ref.1) | copy-start | bytes 2359300
  42.2 38.3 %copy-start.3 = (bf16[1,256,1536]{2,1,0:T(8,128)(2,1)S(1)}, bf16[1,256,1536]{2,1,0:T(8,128)(2,1)}, u32[]{:S(2)}) copy-start(bf16[1,256,1536]{2,1,0:T(8,128)(2,1)} %down_ref.1) | copy-start | bytes 2359300
  42.2 0.8 copy-start.9
  81.9 14.3 %all-to-all-start.5 = ((bf16[32,40,128]{2,1,0:T(8,128)(2,1)}), bf16[32,40,128]{2,1,0:T(8,128)(2,1)S(1)}, u32[]{:S(2)}, u32[]{:S(2)}) async-start(bf16[32,40,128]{2,1,0:T(8,128)(2,1)} %shard_map.173), calls=%async_computation.5 | async-start | bytes 655360 | tf_op jit(solution)/shard_map/all_to_all | solution.py:413
  84.5 11.7 %copy-start.8 = (f32[15,6]{0,1:T(8,128)S(1)}, f32[15,6]{0,1:T(8,128)}, u32[]{:S(2)}) copy-start(f32[15,6]{0,1:T(8,128)} %param.28) | copy-start | bytes 1084
where the time goes:
time: 97.6 us; the launch traced here: 97.1 us
  blocking collectives  43.3 us (44%)
  waiting for transfers between devices  27.9 us (29%)
  Pallas kernels  14 us (14%)
  starting transfers between devices  10.3 us (11%)
    all_to_all x1, blocking collectives, shards(): gathered = lax.all_to_all(spread, chips, 0, 0, tiled=True)  15.2 us
    ppermute x1, waiting for transfers between devices, shards(): far = lax.ppermute(own_o, 'a', [(i, i ^ 2) for i in range(deep)])  15.2 us
    pallas_call x9, Pallas kernels, call(): pl.pallas_call(body, out_shape=out_shape, compiler_params=pltpu.CompilerP...  14 us
    all_to_all x1, blocking collectives, shards(): lax.all_to_all(buffer.reshape(experts, -1, 128), (*chips, 'c'), 0, 0, til...  14 us
    all_to_all x1, blocking collectives, shards(): lax.all_to_all(partial_mix.reshape(plane * tp_count, rows, -1), ('b', 'c'...  7.33 us
    all_to_all x1, blocking collectives, shards(): all_heads = lax.all_to_all(spread_heads, ('b', 'c'), 0, 0, tiled=True)  6.77 us
    ppermute x1, waiting for transfers between devices, shards(): packs.append(lax.ppermute(packs[0], 'a', [(i, i ^ 1) for i in range(deep)]))  6.41 us
    all_to_all x1, waiting for transfers between devices, shards(): back = lax.all_to_all(down, (*chips, 'c', 'tp'), 0, 0, tiled=True)  6.36 us
  transfers between devices with their start and end apart: 5, of which 3 were waited for; matrix products, arithmetic and copies ran while one was open for 0% of the time, Pallas kernels for 7%

commit v1 on v0

--- a/solution.py
+++ b/solution.py
@@ -126,8 +126,7 @@
             both_parts = dot(lhs, state_ref[s, h])
             readout += jnp.where(row_ids == s, both_parts[:rows] + both_parts[rows:], 0.0)
         heads_out = (rms_scale(readout, gain) * gate[:, lanes]).astype(bf16)
-        for g in range(out_ref.shape[0]):
-            out_ref[g, :, lanes] = heads_out
+        out_ref[:, lanes] = heads_out
 
 
 def state_body(forget_ref, value_ref, state_ref, new_ref):
@@ -142,22 +141,25 @@
         ).astype(bf16)
 
 
-def mix_body(x_ref, *refs):
-    *w_refs, out_ref = refs
-    blocks, rows, part = x_ref.shape
-    x = x_ref[...].reshape(blocks * rows, part)
+def mix_body(blocks, *refs):
+    x_refs, w_refs, out_ref = refs[:blocks], refs[blocks:-1], refs[-1]
+    rows, part = x_refs[0].shape
+    x = jnp.concatenate([x_ref[...] for x_ref in x_refs], axis=0)
     ys = [dot_t(x, w_ref[...].reshape(-1, part)) for w_ref in w_refs]
-    if len(ys) == 2:
+    if len(ys) == 4:
         cols = ys[0].shape[1] // 2
-        low = lax.rem(lax.axis_index("a"), 2)
-        ys = [
-            y
-            for high in range(2)
-            for y in core_order(low, *(y[:, high * cols : (high + 1) * cols] for y in ys))
-        ]
-    y = jnp.concatenate(ys, axis=1).astype(bf16).reshape(blocks, rows, -1)
-    for t in range(out_ref.shape[1]):
-        out_ref[:, t] = y
+        low, core = lax.rem(lax.axis_index("a"), 2), lax.axis_index("c")
+        own, near = core_order(core, *ys[:2]), core_order(core, *ys[2:])
+        ys = []
+        for high in range(2):
+            lanes = slice(high * cols, (high + 1) * cols)
+            pairs = [core_order(low, own[c][:, lanes], near[c][:, lanes]) for c in range(2)]
+            ys += [pairs[c][a] for a in range(2) for c in range(2)]
+    y = jnp.concatenate(ys, axis=1).astype(bf16)
+    for i in range(blocks):
+        place = lax.rem(lax.axis_index("b") + i, blocks)
+        for t in range(out_ref.shape[1]):
+            out_ref[place, t] = y[i * rows : (i + 1) * rows]
 
 
 def slots_of(ids, slots, experts):
@@ -182,7 +184,7 @@
     seqs, width = res_ref.shape
     per_row = width // 128
     slots_all = out_ref.shape[0] // per_row
-    experts = deep * blocks
+    experts = deep * blocks * lax.axis_size("c")
     sums = [recv_ref[g].astype(f32).sum(axis=0) for g in range(blocks)]
     mixed = jnp.concatenate(
         [x[:, a * cols : (a + 1) * cols] for a in range(deep) for x in sums], axis=1
@@ -290,7 +292,7 @@
     expert_down,
 ):
     deep, wide, cores, tp_count = (lax.axis_size(a) for a in ("a", "b", "c", "tp"))
-    groups, plane = deep * wide, wide * cores
+    groups = deep * wide
     chips = ("a", "b")
     seqs, width = residual_in.shape
     part = width // tp_count
@@ -318,7 +320,8 @@
             pltpu.SemaphoreType.DMA((7,)),
         ],
     )
-    oth_w = lax.ppermute(own_w, "c", [(i, i ^ 1) for i in range(cores)])
+    swap = [(i, i ^ 1) for i in range(cores)]
+    oth_w = lax.ppermute(own_w, "c", swap)
     if deep == 4:
         far = lax.ppermute(own_o, "a", [(i, i ^ 2) for i in range(deep)])
     gathered = lax.all_to_all(spread, chips, 0, 0, tiled=True)
@@ -332,17 +335,19 @@
     )
     if deep == 4:
         packs = [call(pack_body, sds((2, cols, part), bf16), own_o, far)]
-        packs.append(lax.ppermute(packs[0], "a", [(i, i ^ 1) for i in range(deep)]))
+        near = lax.ppermute(packs[0], "a", [(i, i ^ 1) for i in range(deep)])
+        packs.append(lax.ppermute(packs[0], "c", swap))
+        packs += [near, lax.ppermute(near, "c", swap)]
     else:
-        packs = [lax.all_gather(own_o, "a", axis=0).reshape(deep * cols, part)]
+        packs = [lax.all_gather(own_o, ("a", "c"), axis=0).reshape(-1, part)]
     arrived = lax.all_to_all(
         partial.reshape(groups * tp_count, rows, -1), (*chips, "tp"), 0, 0, tiled=True
     ).reshape(partial.shape)
 
-    spread_heads, forget, value = call(
+    own_heads, forget, value = call(
         read_body,
         [
-            sds((plane, rows, heads * size), bf16),
+            sds((rows, heads * size), bf16),
             sds((rows, heads * size), f32),
             sds((rows, heads * size), f32),
         ],
@@ -351,9 +356,10 @@
         head_gain,
         rec_state,
     )
-    if deep == 4:
-        spread_heads, packs[1] = lax.optimization_barrier((spread_heads, packs[1]))
-    all_heads = lax.all_to_all(spread_heads, ("b", "c"), 0, 0, tiled=True)
+    all_heads = [own_heads] + [
+        lax.ppermute(own_heads, "b", [(i, (i + s) % wide) for i in range(wide)])
+        for s in range(1, wide)
+    ]
 
     per_head = pl.BlockSpec((seqs, 1, size, size), lambda i: (0, i, 0, 0))
     head_lanes = pl.BlockSpec((rows, size), lambda i: (0, i))
@@ -372,10 +378,13 @@
     )
 
     partial_mix = call(
-        mix_body, sds((plane, tp_count, rows, deep * cols), bf16), all_heads, *packs
+        functools.partial(mix_body, wide),
+        sds((wide, tp_count, rows, deep * cores * cols), bf16),
+        *all_heads,
+        *packs,
     )
     mix_home = lax.all_to_all(
-        partial_mix.reshape(plane * tp_count, rows, -1), ("b", "c", "tp"), 0, 0, tiled=True
+        partial_mix.reshape(wide * tp_count, rows, -1), ("b", "tp"), 0, 0, tiled=True
     ).reshape(partial_mix.shape)
 
     experts = groups * cores

time: 97.6 us -> 98.1 us (level)
  blocking collectives: 43.3 us -> 37.6 us
  waiting for transfers between devices: 27.9 us -> 32.3 us
  starting transfers between devices: 10.3 us -> 11.8 us
    all_to_all x2 -> x1, blocking collectives: 14.1 us -> 8.32 us  [shards(): lax.all_to_all(partial_mix.reshape(wide * tp_count, rows, -1), ('b', 'tp'...]
    ppermute x2 -> x5, waiting for transfers between devices: 6.41 us -> 10.7 us  [the longest x1 8.33 us: shards(): near = lax.ppermute(packs[0], 'a', [(i, i ^ 1) for i in range(deep)])]
    ppermute x2 -> x5, starting transfers between devices: 0.56 us -> 2.05 us  [the longest x1 1.48 us: shards(): lax.ppermute(own_heads, 'b', [(i, (i + s) % wide) for i in range(wide)])]
  transfers between devices with their start and end apart: 5 -> 8, of which waited for: 3 -> 4; matrix products, arithmetic and copies ran while one was open for 0% -> 0% of each run, Pallas kernels for 7% -> 7%
where the time goes in v1:
time: 98.1 us; the launch traced here: 97.6 us
  blocking collectives  37.6 us (38%)
  waiting for transfers between devices  32.3 us (33%)
  Pallas kernels  14.4 us (15%)
  starting transfers between devices  11.8 us (12%)
    all_to_all x1, blocking collectives, shards(): gathered = lax.all_to_all(spread, chips, 0, 0, tiled=True)  15.2 us
    ppermute x1, waiting for transfers between devices, shards(): far = lax.ppermute(own_o, 'a', [(i, i ^ 2) for i in range(deep)])  15.2 us
    pallas_call x9, Pallas kernels, call(): pl.pallas_call(body, out_shape=out_shape, compiler_params=pltpu.CompilerP...  14.4 us
    all_to_all x1, blocking collectives, shards(): lax.all_to_all(buffer.reshape(experts, -1, 128), (*chips, 'c'), 0, 0, til...  14.1 us
    ppermute x1, waiting for transfers between devices, shards(): near = lax.ppermute(packs[0], 'a', [(i, i ^ 1) for i in range(deep)])  8.33 us
    all_to_all x1, blocking collectives, shards(): lax.all_to_all(partial_mix.reshape(wide * tp_count, rows, -1), ('b', 'tp'...  8.32 us
    all_to_all x1, waiting for transfers between devices, shards(): back = lax.all_to_all(down, (*chips, 'c', 'tp'), 0, 0, tiled=True)  6.36 us
    all_to_all x1, starting transfers between devices, shards(): lax.all_to_all(partial.reshape(groups * tp_count, rows, -1), (*chips, 'tp...  4.34 us
  transfers between devices with their start and end apart: 8, of which 4 were waited for; matrix products, arithmetic and copies ran while one was open for 0% of the time, Pallas kernels for 7%

profile of v1, /device:TPU:0, one launch (start us, length us, event | category | flops | bytes accessed | tf_op | source)
XLA Modules:
  0.0 97.6 jit_solution(4241539227520401820)
XLA Ops:
  0.6 0.0 copy-start
  0.6 0.0 copy-start.7
  0.7 1.4 %shard_map.167 = (bf16[8,16,768]{2,1,0:T(8,128)(2,1)S(1)}, bf16[4,96,768]{2,1,0:T(8,128)(2,1)S(1)}, bf16[96,768]{1,0:T(8,128)(2,1)S(1)}) custom-call(bf16[15,1536]{1,0:T(8,128)(2,1)} %res_ref.1, f32[1536]{0:T(1024)} %refs_1_.1, bf16[96,768]{1,0:T(8,128)(2,1)} %bitcast.21, bf16[96,768]{1,0:T(8,128)(2,1)} %bitcast.22, bf16[96,768]{1,0:T(8,128)(2,1)} %bitcast.23, ...), custom_call_target="tpu_custom_call" | custom-call | tf_op jit(solution)/shard_map/pallas_call | solution.py:28
  2.1 0.6 collective-permute-start
  2.7 15.2 %all_to_all.25.x_ref = bf16[8,16,768]{2,1,0:T(8,128)(2,1)S(1)} all-to-all(bf16[8,16,768]{2,1,0:T(8,128)(2,1)S(1)} %get-tuple-element.10), channel_id=1, replica_groups=mesh['a'=4,'b'=2,'c'=2,'tp'=2] {'a','b'}, dimensions={0} | all-to-all | bytes 393216 | tf_op jit(solution)/shard_map/all_to_all | solution.py:327
  17.9 0.0 collective-permute-done.oth_ref
  17.9 1.2 %shard_map.168 = bf16[8,2,16,768]{3,2,1,0:T(8,128)(2,1)} custom-call(bf16[8,16,768]{2,1,0:T(8,128)(2,1)S(1)} %all_to_all.25.x_ref, bf16[4,96,768]{2,1,0:T(8,128)(2,1)S(1)} %get-tuple-element.11.own_ref, bf16[4,96,768]{2,1,0:T(8,128)(2,1)S(1)} %collective-permute-done.oth_ref), custom_call_target="tpu_custom_call" | custom-call | tf_op jit(solution)/shard_map/pallas_call | solution.py:28
  19.1 0.0 copy-start.4
  19.1 0.0 copy-start.5
  19.1 0.0 copy-start.6
  19.1 4.3 %all-to-all-start.1 = ((bf16[16,16,768]{2,1,0:T(8,128)(2,1)}), bf16[16,16,768]{2,1,0:T(8,128)(2,1)S(1)}, u32[]{:S(2)}, u32[]{:S(2)}) async-start(bf16[16,16,768]{2,1,0:T(8,128)(2,1)} %bitcast.5), calls=%async_computation.1 | async-start | bytes 786432 | tf_op jit(solution)/shard_map/all_to_all | solution.py:343
  23.4 2.8 %collective-permute-start.2 = (bf16[96,768]{1,0:T(8,128)(2,1)S(1)}, bf16[96,768]{1,0:T(8,128)(2,1)S(1)}, u32[]{:S(2)}, u32[]{:S(2)}) collective-permute-start(bf16[96,768]{1,0:T(8,128)(2,1)S(1)} %get-tuple-element.13.own_ref), channel_id=1, source_target_pairs={{0,16},{8,24},{16,0},{24,8},{1,17},{9,25},{17,1},{25,9},{2,18},{10... | collective-permute-start | bytes 442376 | tf_op jit(solution)/shard_map/ppermute | solution.py:326
  26.3 15.2 %collective-permute-done.2.far_ref = bf16[96,768]{1,0:T(8,128)(2,1)S(1)} collective-permute-done((bf16[96,768]{1,0:T(8,128)(2,1)S(1)}, bf16[96,768]{1,0:T(8,128)(2,1)S(1)}, u32[]{:S(2)}, u32[]{:S(2)}) %collective-permute-start.2) | collective-permute-done | bytes 147488 | tf_op jit(solution)/shard_map/ppermute | solution.py:326
  41.4 0.8 shard_map.170.refs_2_
  42.2 0.0 collective-permute-start.4
  42.2 0.0 collective-permute-start.3
  42.2 8.3 %collective-permute-done.4.refs_4_ = bf16[2,96,768]{2,1,0:T(8,128)(2,1)} collective-permute-done((bf16[2,96,768]{2,1,0:T(8,128)(2,1)}, bf16[2,96,768]{2,1,0:T(8,128)(2,1)}, u32[]{:S(2)}, u32[]{:S(2)}) %collective-permute-start.4) | collective-permute-done | bytes 294944 | tf_op jit(solution)/shard_map/ppermute | solution.py:338
  50.5 0.0 collective-permute-start.5
  50.5 0.0 all-to-all-done.1
  50.5 0.0 copy-start.1
  50.5 0.0 copy-start.2
  50.5 0.0 copy-start.3
  50.6 0.0 copy-done
  50.6 0.0 copy-done.7
  50.6 0.0 copy-start.9
  50.6 0.8 copy-done.9
  51.4 1.1 %shard_map.169 = (bf16[16,768]{1,0:T(8,128)(2,1)S(1)}, f32[16,768]{1,0:T(8,128)S(1)}, f32[16,768]{1,0:T(8,128)S(1)}) custom-call(bf16[8,2,16,768]{3,2,1,0:T(8,128)(2,1)S(1)} %bitcast.13, f32[768]{0:T(1024)S(1)} %copy-done.7, f32[128]{0:T(128)S(1)} %copy-done.9, bf16[15,6,128,128]{3,2,1,0:T(8,128)(2,1)S(1)} %copy-done), custom_call_target="tpu_custom_call" | custom-call | tf_op jit(solution)/shard_map/pallas_call | solution.py:28
  52.4 1.5 %collective-permute-start.1 = (bf16[16,768]{1,0:T(8,128)(2,1)S(1)}, bf16[16,768]{1,0:T(8,128)(2,1)S(1)}, u32[]{:S(2)}, u32[]{:S(2)}) collective-permute-start(bf16[16,768]{1,0:T(8,128)(2,1)S(1)} %get-tuple-element.12.refs_0_), channel_id=1, source_target_pairs={{0,4},{4,0},{1,5},{5,1},{2,6},{6,2},{3,7},{7,3},{8,12},{12,8},{9,1... | collective-permute-start | bytes 73736 | tf_op jit(solution)/shard_map/ppermute | solution.py:360
  53.9 0.0 collective-permute-done.3.refs_3_
  53.9 0.0 collective-permute-done.5.refs_5_
  53.9 2.4 %collective-permute-done.1.refs_1_ = bf16[16,768]{1,0:T(8,128)(2,1)S(1)} collective-permute-done((bf16[16,768]{1,0:T(8,128)(2,1)S(1)}, bf16[16,768]{1,0:T(8,128)(2,1)S(1)}, u32[]{:S(2)}, u32[]{:S(2)}) %collective-permute-start.1) | collective-permute-done | bytes 24608 | tf_op jit(solution)/shard_map/ppermute | solution.py:360
  56.3 1.8 %shard_map.171 = bf16[2,2,16,768]{3,2,1,0:T(8,128)(2,1)S(1)} custom-call(bf16[16,768]{1,0:T(8,128)(2,1)S(1)} %get-tuple-element.12.refs_0_, bf16[16,768]{1,0:T(8,128)(2,1)S(1)} %collective-permute-done.1.refs_1_, bf16[2,96,768]{2,1,0:T(8,128)(2,1)} %shard_map.170.refs_2_, bf16[2,96,768]{2,1,0:T(8,128)(2,1)} %collective-permute-done.3.refs_3_, ...), custom_call_target="tpu_custom_call" | custom-call | tf_op jit(solution)/shard_map/pallas_call | solution.py:28
  58.1 8.3 %all_to_all.26 = bf16[4,16,768]{2,1,0:T(8,128)(2,1)S(1)} all-to-all(bf16[4,16,768]{2,1,0:T(8,128)(2,1)S(1)} %bitcast.16), channel_id=1, replica_groups=mesh['a'=4,'b'=2,'c'=2,'tp'=2] {'b','tp'}, dimensions={0} | all-to-all | bytes 196608 | tf_op jit(solution)/shard_map/all_to_all | solution.py:386
  66.4 0.0 copy-done.4
  66.4 0.0 copy-done.5
  66.4 0.0 copy-done.6
  66.5 0.4 shard_map.172
  66.9 14.1 %all_to_all.27 = bf16[16,72,128]{2,1,0:T(8,128)(2,1)S(1)} all-to-all(bf16[16,72,128]{2,1,0:T(8,128)(2,1)S(1)} %bitcast.17), channel_id=1, replica_groups=mesh['a'=4,'b'=2,'c'=2,'tp'=2] {'a','b','c'}, dimensions={0} | all-to-all | bytes 589824 | tf_op jit(solution)/shard_map/all_to_all | solution.py:403
  80.9 0.0 copy-done.1
  81.0 0.0 copy-done.2
  81.0 0.0 copy-done.3
  81.0 1.4 %shard_map.173 = bf16[32,40,128]{2,1,0:T(8,128)(2,1)} custom-call(bf16[1152,128]{1,0:T(8,128)(2,1)S(1)} %bitcast.14, bf16[1,1536,256]{2,1,0:T(8,128)(2,1)S(1)} %copy-done.1, bf16[1,1536,256]{2,1,0:T(8,128)(2,1)S(1)} %copy-done.2, bf16[1,256,1536]{2,1,0:T(8,128)(2,1)S(1)} %copy-done.3), custom_call_target="tpu_custom_call" | custom-call | tf_op jit(solution)/shard_map/pallas_call | solution.py:28
  82.4 2.6 %all-to-all-start.4 = ((bf16[32,40,128]{2,1,0:T(8,128)(2,1)}), bf16[32,40,128]{2,1,0:T(8,128)(2,1)S(1)}, u32[]{:S(2)}, u32[]{:S(2)}) async-start(bf16[32,40,128]{2,1,0:T(8,128)(2,1)} %shard_map.173), calls=%async_computation.4 | async-start | bytes 655360 | tf_op jit(solution)/shard_map/all_to_all | solution.py:422
  85.0 0.0 copy-start.8
  85.0 5.3 %shard_map.175 = bf16[15,6,128,128]{3,2,1,0:T(8,128)(2,1)} custom-call(f32[16,768]{1,0:T(8,128)S(1)} %get-tuple-element.16.forget_ref, f32[16,768]{1,0:T(8,128)S(1)} %get-tuple-element.17.value_ref, bf16[15,6,128,128]{3,2,1,0:T(8,128)(2,1)S(1)} %copy-done), custom_call_target="tpu_custom_call" | custom-call | flops 10000000 | bytes 5898240 | tf_op jit(solution)/shard_map/pallas_call | solution.py:28
  90.3 6.4 %all-to-all-done.4.back_ref = bf16[32,40,128]{2,1,0:T(8,128)(2,1)S(1)} async-done(((bf16[32,40,128]{2,1,0:T(8,128)(2,1)}), bf16[32,40,128]{2,1,0:T(8,128)(2,1)S(1)}, u32[]{:S(2)}, u32[]{:S(2)}) %all-to-all-start.4) | async-done | bytes 327712 | tf_op jit(solution)/shard_map/all_to_all | solution.py:422
  96.7 0.0 copy-done.8
  96.7 1.0 %shard_map.174 = bf16[15,768]{1,0:T(8,128)(2,1)} custom-call(bf16[32,40,128]{2,1,0:T(8,128)(2,1)S(1)} %all-to-all-done.4.back_ref, s32[6,15]{1,0:T(8,128)S(1)} %bitcast.19, f32[6,15]{1,0:T(8,128)S(1)} %bitcast.20, f32[15,768]{1,0:T(8,128)S(1)} %get-tuple-element.15.own_ref), custom_call_target="tpu_custom_call" | custom-call | tf_op jit(solution)/shard_map/pallas_call | solution.py:28
Async XLA Ops:
  0.6 49.9 %copy-start = (bf16[15,6,128,128]{3,2,1,0:T(8,128)(2,1)S(1)}, bf16[15,6,128,128]{3,2,1,0:T(8,128)(2,1)}, u32[]{:S(2)}) copy-start(bf16[15,6,128,128]{3,2,1,0:T(8,128)(2,1)} %state_ref.3) | copy-start | bytes 8847364
  0.6 49.9 %copy-start.7 = (f32[768]{0:T(1024)S(1)}, f32[768]{0:T(1024)}, u32[]{:S(2)}) copy-start(f32[768]{0:T(1024)} %lower_ref.1) | copy-start | bytes 9220
  2.1 15.8 %collective-permute-start = (bf16[4,96,768]{2,1,0:T(8,128)(2,1)S(1)}, bf16[4,96,768]{2,1,0:T(8,128)(2,1)S(1)}, u32[]{:S(2)}, u32[]{:S(2)}) collective-permute-start(bf16[4,96,768]{2,1,0:T(8,128)(2,1)S(1)} %get-tuple-element.11.own_ref), channel_id=1, source_target_pairs={{0,2},{2,0},{1,3},{3,1},{4,6},{6,4},{5,7},{7,5},{8,10},{10,8},{9,1... | collective-permute-start | bytes 1769480 | tf_op jit(solution)/shard_map/ppermute | solution.py:324
  19.1 47.4 %copy-start.4 = (bf16[15,1536]{1,0:T(8,128)(2,1)S(1)}, bf16[15,1536]{1,0:T(8,128)(2,1)}, u32[]{:S(2)}) copy-start(bf16[15,1536]{1,0:T(8,128)(2,1)} %res_ref.1) | copy-start | bytes 138244
  19.1 47.4 %copy-start.5 = (s32[15,6]{0,1:T(8,128)S(1)}, s32[15,6]{0,1:T(8,128)}, u32[]{:S(2)}) copy-start(s32[15,6]{0,1:T(8,128)} %param.27) | copy-start | bytes 1084
  19.1 47.4 %copy-start.6 = (f32[1536]{0:T(1024)S(1)}, f32[1536]{0:T(1024)}, u32[]{:S(2)}) copy-start(f32[1536]{0:T(1024)} %gain_ref.3) | copy-start | bytes 18436
  19.1 31.4 %all-to-all-start.1 = ((bf16[16,16,768]{2,1,0:T(8,128)(2,1)}), bf16[16,16,768]{2,1,0:T(8,128)(2,1)S(1)}, u32[]{:S(2)}, u32[]{:S(2)}) async-start(bf16[16,16,768]{2,1,0:T(8,128)(2,1)} %bitcast.5), calls=%async_computation.1 | async-start | bytes 786432 | tf_op jit(solution)/shard_map/all_to_all | solution.py:343
  23.4 18.0 %collective-permute-start.2 = (bf16[96,768]{1,0:T(8,128)(2,1)S(1)}, bf16[96,768]{1,0:T(8,128)(2,1)S(1)}, u32[]{:S(2)}, u32[]{:S(2)}) collective-permute-start(bf16[96,768]{1,0:T(8,128)(2,1)S(1)} %get-tuple-element.13.own_ref), channel_id=1, source_target_pairs={{0,16},{8,24},{16,0},{24,8},{1,17},{9,25},{17,1},{25,9},{2,18},{10... | collective-permute-start | bytes 442376 | tf_op jit(solution)/shard_map/ppermute | solution.py:326
  42.2 8.3 %collective-permute-start.4 = (bf16[2,96,768]{2,1,0:T(8,128)(2,1)}, bf16[2,96,768]{2,1,0:T(8,128)(2,1)}, u32[]{:S(2)}, u32[]{:S(2)}) collective-permute-start(bf16[2,96,768]{2,1,0:T(8,128)(2,1)} %shard_map.170.refs_2_), channel_id=1, source_target_pairs={{0,8},{8,0},{16,24},{24,16},{1,9},{9,1},{17,25},{25,17},{2,10},{10... | collective-permute-start | bytes 884744 | tf_op jit(solution)/shard_map/ppermute | solution.py:338
  42.2 11.8 %collective-permute-start.3 = (bf16[2,96,768]{2,1,0:T(8,128)(2,1)}, bf16[2,96,768]{2,1,0:T(8,128)(2,1)}, u32[]{:S(2)}, u32[]{:S(2)}) collective-permute-start(bf16[2,96,768]{2,1,0:T(8,128)(2,1)} %shard_map.170.refs_2_), channel_id=1, source_target_pairs={{0,2},{2,0},{1,3},{3,1},{4,6},{6,4},{5,7},{7,5},{8,10},{10,8},{9,1... | collective-permute-start | bytes 884744 | tf_op jit(solution)/shard_map/ppermute | solution.py:339
  50.5 3.4 %collective-permute-start.5 = (bf16[2,96,768]{2,1,0:T(8,128)(2,1)}, bf16[2,96,768]{2,1,0:T(8,128)(2,1)}, u32[]{:S(2)}, u32[]{:S(2)}) collective-permute-start(bf16[2,96,768]{2,1,0:T(8,128)(2,1)} %collective-permute-done.4.refs_4_), channel_id=1, source_target_pairs={{0,2},{2,0},{1,3},{3,1},{4,6},{6,4},{5,7},{7,5},{8,10},{10,8},{9,1... | collective-permute-start | bytes 884744 | tf_op jit(solution)/shard_map/ppermute | solution.py:340
  50.5 30.4 %copy-start.1 = (bf16[1,1536,256]{2,1,0:T(8,128)(2,1)S(1)}, bf16[1,1536,256]{2,1,0:T(8,128)(2,1)}, u32[]{:S(2)}) copy-start(bf16[1,1536,256]{2,1,0:T(8,128)(2,1)} %gate_ref.1) | copy-start | bytes 2359300
  50.5 30.4 %copy-start.2 = (bf16[1,1536,256]{2,1,0:T(8,128)(2,1)S(1)}, bf16[1,1536,256]{2,1,0:T(8,128)(2,1)}, u32[]{:S(2)}) copy-start(bf16[1,1536,256]{2,1,0:T(8,128)(2,1)} %up_ref.1) | copy-start | bytes 2359300
  50.5 30.4 %copy-start.3 = (bf16[1,256,1536]{2,1,0:T(8,128)(2,1)S(1)}, bf16[1,256,1536]{2,1,0:T(8,128)(2,1)}, u32[]{:S(2)}) copy-start(bf16[1,256,1536]{2,1,0:T(8,128)(2,1)} %down_ref.1) | copy-start | bytes 2359300
  50.6 0.8 copy-start.9
  52.4 3.9 %collective-permute-start.1 = (bf16[16,768]{1,0:T(8,128)(2,1)S(1)}, bf16[16,768]{1,0:T(8,128)(2,1)S(1)}, u32[]{:S(2)}, u32[]{:S(2)}) collective-permute-start(bf16[16,768]{1,0:T(8,128)(2,1)S(1)} %get-tuple-element.12.refs_0_), channel_id=1, source_target_pairs={{0,4},{4,0},{1,5},{5,1},{2,6},{6,2},{3,7},{7,3},{8,12},{12,8},{9,1... | collective-permute-start | bytes 73736 | tf_op jit(solution)/shard_map/ppermute | solution.py:360
  82.4 14.3 %all-to-all-start.4 = ((bf16[32,40,128]{2,1,0:T(8,128)(2,1)}), bf16[32,40,128]{2,1,0:T(8,128)(2,1)S(1)}, u32[]{:S(2)}, u32[]{:S(2)}) async-start(bf16[32,40,128]{2,1,0:T(8,128)(2,1)} %shard_map.173), calls=%async_computation.4 | async-start | bytes 655360 | tf_op jit(solution)/shard_map/all_to_all | solution.py:422
  85.0 11.7 %copy-start.8 = (f32[15,6]{0,1:T(8,128)S(1)}, f32[15,6]{0,1:T(8,128)}, u32[]{:S(2)}) copy-start(f32[15,6]{0,1:T(8,128)} %param.28) | copy-start | bytes 1084

commit v2 on v1

--- a/solution.py
+++ b/solution.py
@@ -142,7 +142,7 @@
 
 
 def mix_body(blocks, *refs):
-    x_refs, w_refs, out_ref = refs[:blocks], refs[blocks:-1], refs[-1]
+    x_refs, w_refs, out_refs = refs[:blocks], refs[blocks:-blocks], refs[-blocks:]
     rows, part = x_refs[0].shape
     x = jnp.concatenate([x_ref[...] for x_ref in x_refs], axis=0)
     ys = [dot_t(x, w_ref[...].reshape(-1, part)) for w_ref in w_refs]
@@ -156,10 +156,8 @@
             pairs = [core_order(low, own[c][:, lanes], near[c][:, lanes]) for c in range(2)]
             ys += [pairs[c][a] for a in range(2) for c in range(2)]
     y = jnp.concatenate(ys, axis=1).astype(bf16)
-    for i in range(blocks):
-        place = lax.rem(lax.axis_index("b") + i, blocks)
-        for t in range(out_ref.shape[1]):
-            out_ref[place, t] = y[i * rows : (i + 1) * rows]
+    for i, out_ref in enumerate(out_refs):
+        out_ref[...] = y[i * rows : (i + 1) * rows]
 
 
 def slots_of(ids, slots, experts):
@@ -177,15 +175,21 @@
     return here, named
 
 
-def dispatch_body(recv_ref, res_ref, gain_ref, ids_ref, out_ref, own_ref, lines):
-    blocks = recv_ref.shape[0]
+def dispatch_body(blocks, *refs):
+    recv_refs, (res_ref, gain_ref, ids_ref, out_ref, own_ref, lines) = refs[:-6], refs[-6:]
     deep = lax.axis_size("a")
-    cols = recv_ref.shape[3] // deep
+    cols = recv_refs[0].shape[1] // deep
     seqs, width = res_ref.shape
     per_row = width // 128
     slots_all = out_ref.shape[0] // per_row
     experts = deep * blocks * lax.axis_size("c")
-    sums = [recv_ref[g].astype(f32).sum(axis=0) for g in range(blocks)]
+    each = len(recv_refs) // blocks
+    sums = [
+        sum(r[...].astype(f32) for r in recv_refs[g * each : (g + 1) * each])
+        for g in range(blocks)
+    ]
+    if blocks == 2:
+        sums = core_order(lax.axis_index("b"), *sums)
     mixed = jnp.concatenate(
         [x[:, a * cols : (a + 1) * cols] for a in range(deep) for x in sums], axis=1
     )[:seqs]
@@ -379,22 +383,29 @@
 
     partial_mix = call(
         functools.partial(mix_body, wide),
-        sds((wide, tp_count, rows, deep * cores * cols), bf16),
+        [sds((rows, deep * cores * cols), bf16)] * wide,
         *all_heads,
         *packs,
     )
-    mix_home = lax.all_to_all(
-        partial_mix.reshape(wide * tp_count, rows, -1), ("b", "tp"), 0, 0, tiled=True
-    ).reshape(partial_mix.shape)
+    mix_home = []
+    for i in range(wide):
+        for t in range(tp_count):
+            perm = [
+                (b * tp_count + p, (b + i) % wide * tp_count + (p + t) % tp_count)
+                for b in range(wide)
+                for p in range(tp_count)
+            ]
+            moved = lax.ppermute(partial_mix[i], ("b", "tp"), perm) if i + t else partial_mix[0]
+            mix_home.append(moved)
 
     experts = groups * cores
     capacity = capacity_of(seqs, route_ids.shape[1], experts)
     assert capacity <= 8
     lines = experts * capacity * width // 128
     buffer, own_mix = call(
-        dispatch_body,
+        functools.partial(dispatch_body, wide),
         [sds((lines, 128), bf16), sds((seqs, part), f32)],
-        mix_home,
+        *mix_home,
         residual_in,
         ffn_gain,
         route_ids.T,

time: 98.1 us -> 96.6 us (0.985)
  blocking collectives: 37.6 us -> 29.4 us
  starting transfers between devices: 11.8 us -> 15.4 us
  waiting for transfers between devices: 32.3 us -> 35.5 us
    all_to_all x1 -> x0, blocking collectives: 8.32 us -> none  [shards(): lax.all_to_all(partial_mix.reshape(wide * tp_count, rows, -1), ('b', 'tp'...]
    ppermute x0 -> x3, starting transfers between devices: none -> 3.55 us  [shards(): lax.ppermute(partial_mix[i], ('b', 'tp'), perm)]
    ppermute x0 -> x3, waiting for transfers between devices: none -> 3.21 us  [shards(): lax.ppermute(partial_mix[i], ('b', 'tp'), perm)]
  transfers between devices with their start and end apart: 8 -> 11, of which waited for: 4 -> 7; matrix products, arithmetic and copies ran while one was open for 0% -> 0% of each run, Pallas kernels for 7% -> 7%
where the time goes in v2:
time: 96.6 us; the launch traced here: 96.2 us
  waiting for transfers between devices  35.5 us (37%)
  blocking collectives  29.4 us (30%)
  starting transfers between devices  15.4 us (16%)
  Pallas kernels  14.4 us (15%)
    all_to_all x1, blocking collectives, shards(): gathered = lax.all_to_all(spread, chips, 0, 0, tiled=True)  15.2 us
    ppermute x1, waiting for transfers between devices, shards(): far = lax.ppermute(own_o, 'a', [(i, i ^ 2) for i in range(deep)])  15.2 us
    pallas_call x9, Pallas kernels, call(): pl.pallas_call(body, out_shape=out_shape, compiler_params=pltpu.CompilerP...  14.4 us
    all_to_all x1, blocking collectives, shards(): lax.all_to_all(buffer.reshape(experts, -1, 128), (*chips, 'c'), 0, 0, til...  14.2 us
    ppermute x1, waiting for transfers between devices, shards(): near = lax.ppermute(packs[0], 'a', [(i, i ^ 1) for i in range(deep)])  8.33 us
    all_to_all x1, waiting for transfers between devices, shards(): back = lax.all_to_all(down, (*chips, 'c', 'tp'), 0, 0, tiled=True)  6.36 us
    all_to_all x1, starting transfers between devices, shards(): lax.all_to_all(partial.reshape(groups * tp_count, rows, -1), (*chips, 'tp...  4.34 us
    ppermute x3, starting transfers between devices, shards(): lax.ppermute(partial_mix[i], ('b', 'tp'), perm)  3.55 us
  transfers between devices with their start and end apart: 11, of which 7 were waited for; matrix products, arithmetic and copies ran while one was open for 0% of the time, Pallas kernels for 7%

profile of v2, /device:TPU:0, one launch (start us, length us, event | category | flops | bytes accessed | tf_op | source)
XLA Modules:
  0.0 96.2 jit_solution(7655192966693795941)
XLA Ops:
  0.6 0.0 copy-start
  0.6 0.0 copy-start.7
  0.7 1.4 %shard_map.167 = (bf16[8,16,768]{2,1,0:T(8,128)(2,1)S(1)}, bf16[4,96,768]{2,1,0:T(8,128)(2,1)S(1)}, bf16[96,768]{1,0:T(8,128)(2,1)S(1)}) custom-call(bf16[15,1536]{1,0:T(8,128)(2,1)} %refs_4_.1, f32[1536]{0:T(1024)} %refs_1_.1, bf16[96,768]{1,0:T(8,128)(2,1)} %bitcast.17, bf16[96,768]{1,0:T(8,128)(2,1)} %bitcast.18, bf16[96,768]{1,0:T(8,128)(2,1)} %bitcast.19, ...), custom_call_target="tpu_custom_call" | custom-call | tf_op jit(solution)/shard_map/pallas_call | solution.py:28
  2.1 0.6 collective-permute-start
  2.7 15.2 %all_to_all.20.x_ref = bf16[8,16,768]{2,1,0:T(8,128)(2,1)S(1)} all-to-all(bf16[8,16,768]{2,1,0:T(8,128)(2,1)S(1)} %get-tuple-element.12), channel_id=1, replica_groups=mesh['a'=4,'b'=2,'c'=2,'tp'=2] {'a','b'}, dimensions={0} | all-to-all | bytes 393216 | tf_op jit(solution)/shard_map/all_to_all | solution.py:331
  17.9 0.0 collective-permute-done.oth_ref
  17.9 1.2 %shard_map.168 = bf16[8,2,16,768]{3,2,1,0:T(8,128)(2,1)} custom-call(bf16[8,16,768]{2,1,0:T(8,128)(2,1)S(1)} %all_to_all.20.x_ref, bf16[4,96,768]{2,1,0:T(8,128)(2,1)S(1)} %get-tuple-element.13.own_ref, bf16[4,96,768]{2,1,0:T(8,128)(2,1)S(1)} %collective-permute-done.oth_ref), custom_call_target="tpu_custom_call" | custom-call | tf_op jit(solution)/shard_map/pallas_call | solution.py:28
  19.1 0.0 copy-start.4
  19.1 0.0 copy-start.5
  19.1 0.0 copy-start.6
  19.1 4.3 %all-to-all-start.1 = ((bf16[16,16,768]{2,1,0:T(8,128)(2,1)}), bf16[16,16,768]{2,1,0:T(8,128)(2,1)S(1)}, u32[]{:S(2)}, u32[]{:S(2)}) async-start(bf16[16,16,768]{2,1,0:T(8,128)(2,1)} %bitcast.5), calls=%async_computation.1 | async-start | bytes 786432 | tf_op jit(solution)/shard_map/all_to_all | solution.py:347
  23.4 2.8 %collective-permute-start.2 = (bf16[96,768]{1,0:T(8,128)(2,1)S(1)}, bf16[96,768]{1,0:T(8,128)(2,1)S(1)}, u32[]{:S(2)}, u32[]{:S(2)}) collective-permute-start(bf16[96,768]{1,0:T(8,128)(2,1)S(1)} %get-tuple-element.15.own_ref), channel_id=1, source_target_pairs={{0,16},{8,24},{16,0},{24,8},{1,17},{9,25},{17,1},{25,9},{2,18},{10... | collective-permute-start | bytes 442376 | tf_op jit(solution)/shard_map/ppermute | solution.py:330
  26.3 15.2 %collective-permute-done.2.far_ref = bf16[96,768]{1,0:T(8,128)(2,1)S(1)} collective-permute-done((bf16[96,768]{1,0:T(8,128)(2,1)S(1)}, bf16[96,768]{1,0:T(8,128)(2,1)S(1)}, u32[]{:S(2)}, u32[]{:S(2)}) %collective-permute-start.2) | collective-permute-done | bytes 147488 | tf_op jit(solution)/shard_map/ppermute | solution.py:330
  41.4 0.7 shard_map.170.refs_2_
  42.2 0.0 collective-permute-start.4
  42.2 0.0 collective-permute-start.3
  42.2 8.3 %collective-permute-done.4.refs_4_ = bf16[2,96,768]{2,1,0:T(8,128)(2,1)} collective-permute-done((bf16[2,96,768]{2,1,0:T(8,128)(2,1)}, bf16[2,96,768]{2,1,0:T(8,128)(2,1)}, u32[]{:S(2)}, u32[]{:S(2)}) %collective-permute-start.4) | collective-permute-done | bytes 294944 | tf_op jit(solution)/shard_map/ppermute | solution.py:342
  50.5 0.0 collective-permute-start.5
  50.5 0.0 all-to-all-done.1
  50.5 0.0 copy-start.1
  50.5 0.0 copy-start.2
  50.5 0.0 copy-start.3
  50.5 0.0 copy-done
  50.6 0.0 copy-done.7
  50.6 0.0 copy-start.9
  50.6 0.8 copy-done.9
  51.4 1.1 %shard_map.169 = (bf16[16,768]{1,0:T(8,128)(2,1)S(1)}, f32[16,768]{1,0:T(8,128)S(1)}, f32[16,768]{1,0:T(8,128)S(1)}) custom-call(bf16[8,2,16,768]{3,2,1,0:T(8,128)(2,1)S(1)} %bitcast.11, f32[768]{0:T(1024)S(1)} %copy-done.7, f32[128]{0:T(128)S(1)} %copy-done.9, bf16[15,6,128,128]{3,2,1,0:T(8,128)(2,1)S(1)} %copy-done), custom_call_target="tpu_custom_call" | custom-call | tf_op jit(solution)/shard_map/pallas_call | solution.py:28
  52.4 1.5 %collective-permute-start.1 = (bf16[16,768]{1,0:T(8,128)(2,1)S(1)}, bf16[16,768]{1,0:T(8,128)(2,1)S(1)}, u32[]{:S(2)}, u32[]{:S(2)}) collective-permute-start(bf16[16,768]{1,0:T(8,128)(2,1)S(1)} %get-tuple-element.14.refs_0_), channel_id=1, source_target_pairs={{0,4},{4,0},{1,5},{5,1},{2,6},{6,2},{3,7},{7,3},{8,12},{12,8},{9,1... | collective-permute-start | bytes 73736 | tf_op jit(solution)/shard_map/ppermute | solution.py:364
  53.9 0.0 collective-permute-done.3.refs_3_
  53.9 0.0 collective-permute-done.5.refs_5_
  53.9 2.4 %collective-permute-done.1.refs_1_ = bf16[16,768]{1,0:T(8,128)(2,1)S(1)} collective-permute-done((bf16[16,768]{1,0:T(8,128)(2,1)S(1)}, bf16[16,768]{1,0:T(8,128)(2,1)S(1)}, u32[]{:S(2)}, u32[]{:S(2)}) %collective-permute-start.1) | collective-permute-done | bytes 24608 | tf_op jit(solution)/shard_map/ppermute | solution.py:364
  56.3 1.8 %shard_map.171 = (bf16[16,768]{1,0:T(8,128)(2,1)S(1)}, bf16[16,768]{1,0:T(8,128)(2,1)S(1)}) custom-call(bf16[16,768]{1,0:T(8,128)(2,1)S(1)} %get-tuple-element.14.refs_0_, bf16[16,768]{1,0:T(8,128)(2,1)S(1)} %collective-permute-done.1.refs_1_, bf16[2,96,768]{2,1,0:T(8,128)(2,1)} %shard_map.170.refs_2_, bf16[2,96,768]{2,1,0:T(8,128)(2,1)} %collective-permute-done.3.refs_3_, ...), custom_call_target="tpu_custom_call" | custom-call | tf_op jit(solution)/shard_map/pallas_call | solution.py:28
  58.1 1.5 %collective-permute-start.6 = (bf16[16,768]{1,0:T(8,128)(2,1)S(1)}, bf16[16,768]{1,0:T(8,128)(2,1)S(1)}, u32[]{:S(2)}, u32[]{:S(2)}) collective-permute-start(bf16[16,768]{1,0:T(8,128)(2,1)S(1)} %get-tuple-element.16.refs_0_), channel_id=1, source_target_pairs={{0,1},{1,0},{4,5},{5,4},{2,3},{3,2},{6,7},{7,6},{8,9},{9,8},{12,13... | collective-permute-start | bytes 73736 | tf_op jit(solution)/shard_map/ppermute | solution.py:398
  59.6 1.4 %collective-permute-start.8 = (bf16[16,768]{1,0:T(8,128)(2,1)S(1)}, bf16[16,768]{1,0:T(8,128)(2,1)S(1)}, u32[]{:S(2)}, u32[]{:S(2)}) collective-permute-start(bf16[16,768]{1,0:T(8,128)(2,1)S(1)} %get-tuple-element.17), channel_id=1, source_target_pairs={{0,5},{1,4},{4,1},{5,0},{2,7},{3,6},{6,3},{7,2},{8,13},{9,12},{12,... | collective-permute-start | bytes 73736 | tf_op jit(solution)/shard_map/ppermute | solution.py:398
  61.1 0.6 collective-permute-start.7
  61.7 0.3 collective-permute-done.6.refs_1_
  62.0 2.4 %collective-permute-done.8.refs_3_ = bf16[16,768]{1,0:T(8,128)(2,1)S(1)} collective-permute-done((bf16[16,768]{1,0:T(8,128)(2,1)S(1)}, bf16[16,768]{1,0:T(8,128)(2,1)S(1)}, u32[]{:S(2)}, u32[]{:S(2)}) %collective-permute-start.8) | collective-permute-done | bytes 24608 | tf_op jit(solution)/shard_map/ppermute | solution.py:398
  64.4 0.5 collective-permute-done.7.refs_2_
  64.9 0.0 copy-done.4
  64.9 0.0 copy-done.5
  64.9 0.0 copy-done.6
  64.9 0.4 shard_map.172
  65.3 14.2 %all_to_all.21 = bf16[16,72,128]{2,1,0:T(8,128)(2,1)S(1)} all-to-all(bf16[16,72,128]{2,1,0:T(8,128)(2,1)S(1)} %bitcast.13), channel_id=1, replica_groups=mesh['a'=4,'b'=2,'c'=2,'tp'=2] {'a','b','c'}, dimensions={0} | all-to-all | bytes 589824 | tf_op jit(solution)/shard_map/all_to_all | solution.py:414
  79.5 0.0 copy-done.1
  79.5 0.0 copy-done.2
  79.5 0.0 copy-done.3
  79.5 1.4 %shard_map.173 = bf16[32,40,128]{2,1,0:T(8,128)(2,1)} custom-call(bf16[1152,128]{1,0:T(8,128)(2,1)S(1)} %bitcast.12, bf16[1,1536,256]{2,1,0:T(8,128)(2,1)S(1)} %copy-done.1, bf16[1,1536,256]{2,1,0:T(8,128)(2,1)S(1)} %copy-done.2, bf16[1,256,1536]{2,1,0:T(8,128)(2,1)S(1)} %copy-done.3), custom_call_target="tpu_custom_call" | custom-call | tf_op jit(solution)/shard_map/pallas_call | solution.py:28
  80.9 2.6 %all-to-all-start.3 = ((bf16[32,40,128]{2,1,0:T(8,128)(2,1)}), bf16[32,40,128]{2,1,0:T(8,128)(2,1)S(1)}, u32[]{:S(2)}, u32[]{:S(2)}) async-start(bf16[32,40,128]{2,1,0:T(8,128)(2,1)} %shard_map.173), calls=%async_computation.3 | async-start | bytes 655360 | tf_op jit(solution)/shard_map/all_to_all | solution.py:433
  83.5 0.0 copy-start.8
  83.5 5.3 %shard_map.175 = bf16[15,6,128,128]{3,2,1,0:T(8,128)(2,1)} custom-call(f32[16,768]{1,0:T(8,128)S(1)} %get-tuple-element.20.forget_ref, f32[16,768]{1,0:T(8,128)S(1)} %get-tuple-element.21.value_ref, bf16[15,6,128,128]{3,2,1,0:T(8,128)(2,1)S(1)} %copy-done), custom_call_target="tpu_custom_call" | custom-call | flops 10000000 | bytes 5898240 | tf_op jit(solution)/shard_map/pallas_call | solution.py:28
  88.8 6.4 %all-to-all-done.3.back_ref = bf16[32,40,128]{2,1,0:T(8,128)(2,1)S(1)} async-done(((bf16[32,40,128]{2,1,0:T(8,128)(2,1)}), bf16[32,40,128]{2,1,0:T(8,128)(2,1)S(1)}, u32[]{:S(2)}, u32[]{:S(2)}) %all-to-all-start.3) | async-done | bytes 327712 | tf_op jit(solution)/shard_map/all_to_all | solution.py:433
  95.2 0.0 copy-done.8
  95.2 1.0 %shard_map.174 = bf16[15,768]{1,0:T(8,128)(2,1)} custom-call(bf16[32,40,128]{2,1,0:T(8,128)(2,1)S(1)} %all-to-all-done.3.back_ref, s32[6,15]{1,0:T(8,128)S(1)} %bitcast.15, f32[6,15]{1,0:T(8,128)S(1)} %bitcast.16, f32[15,768]{1,0:T(8,128)S(1)} %get-tuple-element.19.own_ref), custom_call_target="tpu_custom_call" | custom-call | tf_op jit(solution)/shard_map/pallas_call | solution.py:28
Async XLA Ops:
  0.6 49.9 %copy-start = (bf16[15,6,128,128]{3,2,1,0:T(8,128)(2,1)S(1)}, bf16[15,6,128,128]{3,2,1,0:T(8,128)(2,1)}, u32[]{:S(2)}) copy-start(bf16[15,6,128,128]{3,2,1,0:T(8,128)(2,1)} %state_ref.3) | copy-start | bytes 8847364
  0.6 49.9 %copy-start.7 = (f32[768]{0:T(1024)S(1)}, f32[768]{0:T(1024)}, u32[]{:S(2)}) copy-start(f32[768]{0:T(1024)} %lower_ref.1) | copy-start | bytes 9220
  2.1 15.8 %collective-permute-start = (bf16[4,96,768]{2,1,0:T(8,128)(2,1)S(1)}, bf16[4,96,768]{2,1,0:T(8,128)(2,1)S(1)}, u32[]{:S(2)}, u32[]{:S(2)}) collective-permute-start(bf16[4,96,768]{2,1,0:T(8,128)(2,1)S(1)} %get-tuple-element.13.own_ref), channel_id=1, source_target_pairs={{0,2},{2,0},{1,3},{3,1},{4,6},{6,4},{5,7},{7,5},{8,10},{10,8},{9,1... | collective-permute-start | bytes 1769480 | tf_op jit(solution)/shard_map/ppermute | solution.py:328
  19.1 45.8 %copy-start.4 = (bf16[15,1536]{1,0:T(8,128)(2,1)S(1)}, bf16[15,1536]{1,0:T(8,128)(2,1)}, u32[]{:S(2)}) copy-start(bf16[15,1536]{1,0:T(8,128)(2,1)} %refs_4_.1) | copy-start | bytes 138244
  19.1 45.8 %copy-start.5 = (s32[15,6]{0,1:T(8,128)S(1)}, s32[15,6]{0,1:T(8,128)}, u32[]{:S(2)}) copy-start(s32[15,6]{0,1:T(8,128)} %param.27) | copy-start | bytes 1084
  19.1 45.8 %copy-start.6 = (f32[1536]{0:T(1024)S(1)}, f32[1536]{0:T(1024)}, u32[]{:S(2)}) copy-start(f32[1536]{0:T(1024)} %refs_5_.1) | copy-start | bytes 18436
  19.1 31.4 %all-to-all-start.1 = ((bf16[16,16,768]{2,1,0:T(8,128)(2,1)}), bf16[16,16,768]{2,1,0:T(8,128)(2,1)S(1)}, u32[]{:S(2)}, u32[]{:S(2)}) async-start(bf16[16,16,768]{2,1,0:T(8,128)(2,1)} %bitcast.5), calls=%async_computation.1 | async-start | bytes 786432 | tf_op jit(solution)/shard_map/all_to_all | solution.py:347
  23.4 18.0 %collective-permute-start.2 = (bf16[96,768]{1,0:T(8,128)(2,1)S(1)}, bf16[96,768]{1,0:T(8,128)(2,1)S(1)}, u32[]{:S(2)}, u32[]{:S(2)}) collective-permute-start(bf16[96,768]{1,0:T(8,128)(2,1)S(1)} %get-tuple-element.15.own_ref), channel_id=1, source_target_pairs={{0,16},{8,24},{16,0},{24,8},{1,17},{9,25},{17,1},{25,9},{2,18},{10... | collective-permute-start | bytes 442376 | tf_op jit(solution)/shard_map/ppermute | solution.py:330
  42.2 8.3 %collective-permute-start.4 = (bf16[2,96,768]{2,1,0:T(8,128)(2,1)}, bf16[2,96,768]{2,1,0:T(8,128)(2,1)}, u32[]{:S(2)}, u32[]{:S(2)}) collective-permute-start(bf16[2,96,768]{2,1,0:T(8,128)(2,1)} %shard_map.170.refs_2_), channel_id=1, source_target_pairs={{0,8},{8,0},{16,24},{24,16},{1,9},{9,1},{17,25},{25,17},{2,10},{10... | collective-permute-start | bytes 884744 | tf_op jit(solution)/shard_map/ppermute | solution.py:342
  42.2 11.8 %collective-permute-start.3 = (bf16[2,96,768]{2,1,0:T(8,128)(2,1)}, bf16[2,96,768]{2,1,0:T(8,128)(2,1)}, u32[]{:S(2)}, u32[]{:S(2)}) collective-permute-start(bf16[2,96,768]{2,1,0:T(8,128)(2,1)} %shard_map.170.refs_2_), channel_id=1, source_target_pairs={{0,2},{2,0},{1,3},{3,1},{4,6},{6,4},{5,7},{7,5},{8,10},{10,8},{9,1... | collective-permute-start | bytes 884744 | tf_op jit(solution)/shard_map/ppermute | solution.py:343
  50.5 3.4 %collective-permute-start.5 = (bf16[2,96,768]{2,1,0:T(8,128)(2,1)}, bf16[2,96,768]{2,1,0:T(8,128)(2,1)}, u32[]{:S(2)}, u32[]{:S(2)}) collective-permute-start(bf16[2,96,768]{2,1,0:T(8,128)(2,1)} %collective-permute-done.4.refs_4_), channel_id=1, source_target_pairs={{0,2},{2,0},{1,3},{3,1},{4,6},{6,4},{5,7},{7,5},{8,10},{10,8},{9,1... | collective-permute-start | bytes 884744 | tf_op jit(solution)/shard_map/ppermute | solution.py:344
  50.5 29.0 %copy-start.1 = (bf16[1,1536,256]{2,1,0:T(8,128)(2,1)S(1)}, bf16[1,1536,256]{2,1,0:T(8,128)(2,1)}, u32[]{:S(2)}) copy-start(bf16[1,1536,256]{2,1,0:T(8,128)(2,1)} %gate_ref.1) | copy-start | bytes 2359300
  50.5 29.0 %copy-start.2 = (bf16[1,1536,256]{2,1,0:T(8,128)(2,1)S(1)}, bf16[1,1536,256]{2,1,0:T(8,128)(2,1)}, u32[]{:S(2)}) copy-start(bf16[1,1536,256]{2,1,0:T(8,128)(2,1)} %up_ref.1) | copy-start | bytes 2359300
  50.5 29.0 %copy-start.3 = (bf16[1,256,1536]{2,1,0:T(8,128)(2,1)S(1)}, bf16[1,256,1536]{2,1,0:T(8,128)(2,1)}, u32[]{:S(2)}) copy-start(bf16[1,256,1536]{2,1,0:T(8,128)(2,1)} %down_ref.1) | copy-start | bytes 2359300
  50.6 0.8 copy-start.9
  52.4 3.9 %collective-permute-start.1 = (bf16[16,768]{1,0:T(8,128)(2,1)S(1)}, bf16[16,768]{1,0:T(8,128)(2,1)S(1)}, u32[]{:S(2)}, u32[]{:S(2)}) collective-permute-start(bf16[16,768]{1,0:T(8,128)(2,1)S(1)} %get-tuple-element.14.refs_0_), channel_id=1, source_target_pairs={{0,4},{4,0},{1,5},{5,1},{2,6},{6,2},{3,7},{7,3},{8,12},{12,8},{9,1... | collective-permute-start | bytes 73736 | tf_op jit(solution)/shard_map/ppermute | solution.py:364
  58.1 3.9 %collective-permute-start.6 = (bf16[16,768]{1,0:T(8,128)(2,1)S(1)}, bf16[16,768]{1,0:T(8,128)(2,1)S(1)}, u32[]{:S(2)}, u32[]{:S(2)}) collective-permute-start(bf16[16,768]{1,0:T(8,128)(2,1)S(1)} %get-tuple-element.16.refs_0_), channel_id=1, source_target_pairs={{0,1},{1,0},{4,5},{5,4},{2,3},{3,2},{6,7},{7,6},{8,9},{9,8},{12,13... | collective-permute-start | bytes 73736 | tf_op jit(solution)/shard_map/ppermute | solution.py:398
  59.6 4.7 %collective-permute-start.8 = (bf16[16,768]{1,0:T(8,128)(2,1)S(1)}, bf16[16,768]{1,0:T(8,128)(2,1)S(1)}, u32[]{:S(2)}, u32[]{:S(2)}) collective-permute-start(bf16[16,768]{1,0:T(8,128)(2,1)S(1)} %get-tuple-element.17), channel_id=1, source_target_pairs={{0,5},{1,4},{4,1},{5,0},{2,7},{3,6},{6,3},{7,2},{8,13},{9,12},{12,... | collective-permute-start | bytes 73736 | tf_op jit(solution)/shard_map/ppermute | solution.py:398
  61.1 3.8 %collective-permute-start.7 = (bf16[16,768]{1,0:T(8,128)(2,1)S(1)}, bf16[16,768]{1,0:T(8,128)(2,1)S(1)}, u32[]{:S(2)}, u32[]{:S(2)}) collective-permute-start(bf16[16,768]{1,0:T(8,128)(2,1)S(1)} %get-tuple-element.17), channel_id=1, source_target_pairs={{0,4},{1,5},{4,0},{5,1},{2,6},{3,7},{6,2},{7,3},{8,12},{9,13},{12,... | collective-permute-start | bytes 73736 | tf_op jit(solution)/shard_map/ppermute | solution.py:398
  80.9 14.3 %all-to-all-start.3 = ((bf16[32,40,128]{2,1,0:T(8,128)(2,1)}), bf16[32,40,128]{2,1,0:T(8,128)(2,1)S(1)}, u32[]{:S(2)}, u32[]{:S(2)}) async-start(bf16[32,40,128]{2,1,0:T(8,128)(2,1)} %shard_map.173), calls=%async_computation.3 | async-start | bytes 655360 | tf_op jit(solution)/shard_map/all_to_all | solution.py:433
  83.5 11.7 %copy-start.8 = (f32[15,6]{0,1:T(8,128)S(1)}, f32[15,6]{0,1:T(8,128)}, u32[]{:S(2)}) copy-start(f32[15,6]{0,1:T(8,128)} %param.28) | copy-start | bytes 1084

commit v3 on v2

--- a/solution.py
+++ b/solution.py
@@ -146,14 +146,15 @@
     rows, part = x_refs[0].shape
     x = jnp.concatenate([x_ref[...] for x_ref in x_refs], axis=0)
     ys = [dot_t(x, w_ref[...].reshape(-1, part)) for w_ref in w_refs]
-    if len(ys) == 4:
-        cols = ys[0].shape[1] // 2
-        low, core = lax.rem(lax.axis_index("a"), 2), lax.axis_index("c")
-        own, near = core_order(core, *ys[:2]), core_order(core, *ys[2:])
+    if len(ys) == 6:
+        cols = ys[2].shape[1]
+        high, low = lax.axis_index("a") // 2, lax.rem(lax.axis_index("a"), 2)
+        own, side, past = (core_order(lax.axis_index("c"), *ys[i : i + 2]) for i in (0, 2, 4))
+        near = [core_order(high, side[c], past[c]) for c in range(2)]
         ys = []
-        for high in range(2):
-            lanes = slice(high * cols, (high + 1) * cols)
-            pairs = [core_order(low, own[c][:, lanes], near[c][:, lanes]) for c in range(2)]
+        for h in range(2):
+            lanes = slice(h * cols, (h + 1) * cols)
+            pairs = [core_order(low, own[c][:, lanes], near[c][h]) for c in range(2)]
             ys += [pairs[c][a] for a in range(2) for c in range(2)]
     y = jnp.concatenate(ys, axis=1).astype(bf16)
     for i, out_ref in enumerate(out_refs):
@@ -328,6 +329,7 @@
     oth_w = lax.ppermute(own_w, "c", swap)
     if deep == 4:
         far = lax.ppermute(own_o, "a", [(i, i ^ 2) for i in range(deep)])
+        side = lax.ppermute(own_o, "a", [(i, i ^ 1) for i in range(deep)])
     gathered = lax.all_to_all(spread, chips, 0, 0, tiled=True)
 
     partial = call(
@@ -339,8 +341,9 @@
     )
     if deep == 4:
         packs = [call(pack_body, sds((2, cols, part), bf16), own_o, far)]
-        near = lax.ppermute(packs[0], "a", [(i, i ^ 1) for i in range(deep)])
+        near = lax.ppermute(far, "a", [(i, i ^ 1) for i in range(deep)])
         packs.append(lax.ppermute(packs[0], "c", swap))
+        packs += [side, lax.ppermute(side, "c", swap)]
         packs += [near, lax.ppermute(near, "c", swap)]
     else:
         packs = [lax.all_gather(own_o, ("a", "c"), axis=0).reshape(-1, part)]

time: 96.6 us -> 93.3 us (0.966)
  waiting for transfers between devices: 35.5 us -> 28 us
  starting transfers between devices: 15.4 us -> 17.3 us
  Pallas kernels: 14.4 us -> 16 us
    ppermute x1 -> x3, waiting for transfers between devices: 8.33 us -> 3.08 us  [the longest x1 3.08 us: shards(): near = lax.ppermute(far, 'a', [(i, i ^ 1) for i in range(deep)])]
    ppermute x1 -> x3, starting transfers between devices: 0.01 us -> 1.98 us  [the longest x1 1.46 us: shards(): side = lax.ppermute(own_o, 'a', [(i, i ^ 1) for i in range(deep)])]
    pallas_call x9, Pallas kernels: 14.4 us -> 16 us  [call(): pl.pallas_call(body, out_shape=out_shape, compiler_params=pltpu.CompilerP...]
    ppermute x1, waiting for transfers between devices: 15.2 us -> 13.7 us  [shards(): far = lax.ppermute(own_o, 'a', [(i, i ^ 2) for i in range(deep)])]
  transfers between devices with their start and end apart: 11 -> 13, of which waited for: 7 -> 7; matrix products, arithmetic and copies ran while one was open for 0% -> 0% of each run, Pallas kernels for 7% -> 9%
where the time goes in v3:
time: 93.3 us; the launch traced here: 92.8 us
  blocking collectives  29.1 us (31%)
  waiting for transfers between devices  28 us (30%)
  starting transfers between devices  17.3 us (19%)
  Pallas kernels  16 us (17%)
  local copies, waits for them, and re-layouts  1.65 us (2%)
    pallas_call x9, Pallas kernels, call(): pl.pallas_call(body, out_shape=out_shape, compiler_params=pltpu.CompilerP...  16 us
    all_to_all x1, blocking collectives, shards(): gathered = lax.all_to_all(spread, chips, 0, 0, tiled=True)  15.2 us
    all_to_all x1, blocking collectives, shards(): lax.all_to_all(buffer.reshape(experts, -1, 128), (*chips, 'c'), 0, 0, til...  13.9 us
    ppermute x1, waiting for transfers between devices, shards(): far = lax.ppermute(own_o, 'a', [(i, i ^ 2) for i in range(deep)])  13.7 us
    all_to_all x1, waiting for transfers between devices, shards(): back = lax.all_to_all(down, (*chips, 'c', 'tp'), 0, 0, tiled=True)  5.58 us
    all_to_all x1, starting transfers between devices, shards(): lax.all_to_all(partial.reshape(groups * tp_count, rows, -1), (*chips, 'tp...  4.34 us
    ppermute x3, starting transfers between devices, shards(): lax.ppermute(partial_mix[i], ('b', 'tp'), perm)  3.55 us
    ppermute x3, waiting for transfers between devices, shards(): lax.ppermute(partial_mix[i], ('b', 'tp'), perm)  3.22 us
  transfers between devices with their start and end apart: 13, of which 7 were waited for; matrix products, arithmetic and copies ran while one was open for 0% of the time, Pallas kernels for 9%

profile of v3, /device:TPU:0, one launch (start us, length us, event | category | flops | bytes accessed | tf_op | source)
XLA Modules:
  0.0 92.8 jit_solution(6379844252739039944)
XLA Ops:
  0.6 0.0 copy-start
  0.6 0.0 copy-start.11
  0.7 2.1 %shard_map.167 = (bf16[8,16,768]{2,1,0:T(8,128)(2,1)S(1)}, bf16[4,96,768]{2,1,0:T(8,128)(2,1)S(1)}, bf16[96,768]{1,0:T(8,128)(2,1)}) custom-call(bf16[15,1536]{1,0:T(8,128)(2,1)} %refs_4_.1, f32[1536]{0:T(1024)} %refs_1_.1, bf16[96,768]{1,0:T(8,128)(2,1)} %bitcast.17, bf16[96,768]{1,0:T(8,128)(2,1)} %bitcast.18, bf16[96,768]{1,0:T(8,128)(2,1)} %bitcast.19, ...), custom_call_target="tpu_custom_call" | custom-call | tf_op jit(solution)/shard_map/pallas_call | solution.py:28
  2.8 0.6 collective-permute-start
  3.3 15.2 %all_to_all.20.x_ref = bf16[8,16,768]{2,1,0:T(8,128)(2,1)S(1)} all-to-all(bf16[8,16,768]{2,1,0:T(8,128)(2,1)S(1)} %get-tuple-element.12), channel_id=1, replica_groups=mesh['a'=4,'b'=2,'c'=2,'tp'=2] {'a','b'}, dimensions={0} | all-to-all | bytes 393216 | tf_op jit(solution)/shard_map/all_to_all | solution.py:333
  18.5 0.0 collective-permute-done.oth_ref
  18.5 1.2 %shard_map.168 = bf16[8,2,16,768]{3,2,1,0:T(8,128)(2,1)} custom-call(bf16[8,16,768]{2,1,0:T(8,128)(2,1)S(1)} %all_to_all.20.x_ref, bf16[4,96,768]{2,1,0:T(8,128)(2,1)S(1)} %get-tuple-element.13.own_ref, bf16[4,96,768]{2,1,0:T(8,128)(2,1)S(1)} %collective-permute-done.oth_ref), custom_call_target="tpu_custom_call" | custom-call | tf_op jit(solution)/shard_map/pallas_call | solution.py:28
  19.7 0.0 copy-start.4
  19.7 0.0 copy-start.9
  19.8 4.3 %all-to-all-start.1 = ((bf16[16,16,768]{2,1,0:T(8,128)(2,1)}), bf16[16,16,768]{2,1,0:T(8,128)(2,1)S(1)}, u32[]{:S(2)}, u32[]{:S(2)}) async-start(bf16[16,16,768]{2,1,0:T(8,128)(2,1)} %bitcast.5), calls=%async_computation.1 | async-start | bytes 786432 | tf_op jit(solution)/shard_map/all_to_all | solution.py:350
  24.1 2.8 %collective-permute-start.2 = (bf16[96,768]{1,0:T(8,128)(2,1)}, bf16[96,768]{1,0:T(8,128)(2,1)S(1)}, u32[]{:S(2)}, u32[]{:S(2)}) collective-permute-start(bf16[96,768]{1,0:T(8,128)(2,1)} %get-tuple-element.15.own_ref), channel_id=1, source_target_pairs={{0,16},{8,24},{16,0},{24,8},{1,17},{9,25},{17,1},{25,9},{2,18},{10... | collective-permute-start | bytes 442376 | tf_op jit(solution)/shard_map/ppermute | solution.py:331
  26.9 1.5 %collective-permute-start.4 = (bf16[96,768]{1,0:T(8,128)(2,1)}, bf16[96,768]{1,0:T(8,128)(2,1)S(1)}, u32[]{:S(2)}, u32[]{:S(2)}) collective-permute-start(bf16[96,768]{1,0:T(8,128)(2,1)} %get-tuple-element.15.own_ref), channel_id=1, source_target_pairs={{0,8},{8,0},{16,24},{24,16},{1,9},{9,1},{17,25},{25,17},{2,10},{10... | collective-permute-start | bytes 442376 | tf_op jit(solution)/shard_map/ppermute | solution.py:332
  28.4 13.7 %collective-permute-done.2.far_ref = bf16[96,768]{1,0:T(8,128)(2,1)S(1)} collective-permute-done((bf16[96,768]{1,0:T(8,128)(2,1)}, bf16[96,768]{1,0:T(8,128)(2,1)S(1)}, u32[]{:S(2)}, u32[]{:S(2)}) %collective-permute-start.2) | collective-permute-done | bytes 147488 | tf_op jit(solution)/shard_map/ppermute | solution.py:331
  42.1 0.0 collective-permute-start.6
  42.1 1.7 %shard_map.170.refs_2_ = bf16[2,96,768]{2,1,0:T(8,128)(2,1)} custom-call(bf16[96,768]{1,0:T(8,128)(2,1)} %get-tuple-element.15.own_ref, bf16[96,768]{1,0:T(8,128)(2,1)S(1)} %collective-permute-done.2.far_ref), custom_call_target="tpu_custom_call" | custom-call | tf_op jit(solution)/shard_map/pallas_call | solution.py:28
  43.7 0.0 collective-permute-start.3
  43.7 0.0 collective-permute-done.4.refs_4_
  43.8 0.5 collective-permute-start.5
  44.3 3.1 %collective-permute-done.6.refs_6_ = bf16[96,768]{1,0:T(8,128)(2,1)} collective-permute-done((bf16[96,768]{1,0:T(8,128)(2,1)S(1)}, bf16[96,768]{1,0:T(8,128)(2,1)}, u32[]{:S(2)}, u32[]{:S(2)}) %collective-permute-start.6) | collective-permute-done | bytes 147488 | tf_op jit(solution)/shard_map/ppermute | solution.py:344
  47.3 0.0 collective-permute-start.7
  47.3 0.0 all-to-all-done.1
  47.3 0.0 copy-start.1
  47.3 0.0 copy-start.2
  47.4 0.0 copy-start.3
  47.4 0.0 copy-done
  47.4 0.0 copy-done.11
  47.4 0.0 copy-start.13
  47.4 0.8 copy-done.13
  48.2 1.1 %shard_map.169 = (bf16[16,768]{1,0:T(8,128)(2,1)S(1)}, f32[16,768]{1,0:T(8,128)S(1)}, f32[16,768]{1,0:T(8,128)S(1)}) custom-call(bf16[8,2,16,768]{3,2,1,0:T(8,128)(2,1)S(1)} %bitcast.11, f32[768]{0:T(1024)S(1)} %copy-done.11, f32[128]{0:T(128)S(1)} %copy-done.13, bf16[15,6,128,128]{3,2,1,0:T(8,128)(2,1)S(1)} %copy-done), custom_call_target="tpu_custom_call" | custom-call | tf_op jit(solution)/shard_map/pallas_call | solution.py:28
  49.3 0.0 copy-start.5
  49.3 0.0 copy-start.7
  49.3 1.5 %collective-permute-start.1 = (bf16[16,768]{1,0:T(8,128)(2,1)S(1)}, bf16[16,768]{1,0:T(8,128)(2,1)S(1)}, u32[]{:S(2)}, u32[]{:S(2)}) collective-permute-start(bf16[16,768]{1,0:T(8,128)(2,1)S(1)} %get-tuple-element.14.refs_0_), channel_id=1, source_target_pairs={{0,4},{4,0},{1,5},{5,1},{2,6},{6,2},{3,7},{7,3},{8,12},{12,8},{9,1... | collective-permute-start | bytes 73736 | tf_op jit(solution)/shard_map/ppermute | solution.py:367
  50.8 0.0 collective-permute-done.5.refs_5_
  50.8 0.0 collective-permute-done.7.refs_7_
  50.8 0.0 collective-permute-done.3.refs_3_
  50.8 2.4 %collective-permute-done.1.refs_1_ = bf16[16,768]{1,0:T(8,128)(2,1)S(1)} collective-permute-done((bf16[16,768]{1,0:T(8,128)(2,1)S(1)}, bf16[16,768]{1,0:T(8,128)(2,1)S(1)}, u32[]{:S(2)}, u32[]{:S(2)}) %collective-permute-start.1) | collective-permute-done | bytes 24608 | tf_op jit(solution)/shard_map/ppermute | solution.py:367
  53.2 1.8 %shard_map.171 = (bf16[16,768]{1,0:T(8,128)(2,1)S(1)}, bf16[16,768]{1,0:T(8,128)(2,1)S(1)}) custom-call(bf16[16,768]{1,0:T(8,128)(2,1)S(1)} %get-tuple-element.14.refs_0_, bf16[16,768]{1,0:T(8,128)(2,1)S(1)} %collective-permute-done.1.refs_1_, bf16[2,96,768]{2,1,0:T(8,128)(2,1)} %shard_map.170.refs_2_, bf16[2,96,768]{2,1,0:T(8,128)(2,1)} %collective-permute-done.3.refs_3_, ...), custom_call_target="tpu_custom_call" | custom-call | tf_op jit(solution)/shard_map/pallas_call | solution.py:28
  55.0 1.5 %collective-permute-start.8 = (bf16[16,768]{1,0:T(8,128)(2,1)S(1)}, bf16[16,768]{1,0:T(8,128)(2,1)S(1)}, u32[]{:S(2)}, u32[]{:S(2)}) collective-permute-start(bf16[16,768]{1,0:T(8,128)(2,1)S(1)} %get-tuple-element.16.refs_0_), channel_id=1, source_target_pairs={{0,1},{1,0},{4,5},{5,4},{2,3},{3,2},{6,7},{7,6},{8,9},{9,8},{12,13... | collective-permute-start | bytes 73736 | tf_op jit(solution)/shard_map/ppermute | solution.py:401
  56.6 1.4 %collective-permute-start.10 = (bf16[16,768]{1,0:T(8,128)(2,1)S(1)}, bf16[16,768]{1,0:T(8,128)(2,1)S(1)}, u32[]{:S(2)}, u32[]{:S(2)}) collective-permute-start(bf16[16,768]{1,0:T(8,128)(2,1)S(1)} %get-tuple-element.17), channel_id=1, source_target_pairs={{0,5},{1,4},{4,1},{5,0},{2,7},{3,6},{6,3},{7,2},{8,13},{9,12},{12,... | collective-permute-start | bytes 73736 | tf_op jit(solution)/shard_map/ppermute | solution.py:401
  58.0 0.6 collective-permute-start.9
  58.6 0.3 collective-permute-done.8.refs_1_
  58.9 2.4 %collective-permute-done.10.refs_3_ = bf16[16,768]{1,0:T(8,128)(2,1)S(1)} collective-permute-done((bf16[16,768]{1,0:T(8,128)(2,1)S(1)}, bf16[16,768]{1,0:T(8,128)(2,1)S(1)}, u32[]{:S(2)}, u32[]{:S(2)}) %collective-permute-start.10) | collective-permute-done | bytes 24608 | tf_op jit(solution)/shard_map/ppermute | solution.py:401
  61.3 0.5 collective-permute-done.9.refs_2_
  61.8 0.0 copy-done.4
  61.8 0.0 copy-done.9
  61.8 0.0 copy-done.10
  61.8 0.4 shard_map.172
  62.2 13.9 %all_to_all.21 = bf16[16,72,128]{2,1,0:T(8,128)(2,1)S(1)} all-to-all(bf16[16,72,128]{2,1,0:T(8,128)(2,1)S(1)} %bitcast.13), channel_id=1, replica_groups=mesh['a'=4,'b'=2,'c'=2,'tp'=2] {'a','b','c'}, dimensions={0} | all-to-all | bytes 589824 | tf_op jit(solution)/shard_map/all_to_all | solution.py:417
  76.1 0.0 copy-done.5
  76.1 0.0 copy-done.7
  76.1 0.0 copy-done.1
  76.1 0.0 copy-done.2
  76.1 0.0 copy-done.3
  76.1 0.0 copy-start.6
  76.2 1.4 %shard_map.173 = bf16[32,40,128]{2,1,0:T(8,128)(2,1)} custom-call(bf16[1152,128]{1,0:T(8,128)(2,1)S(1)} %bitcast.12, bf16[1,1536,256]{2,1,0:T(8,128)(2,1)S(1)} %copy-done.1, bf16[1,1536,256]{2,1,0:T(8,128)(2,1)S(1)} %copy-done.2, bf16[1,256,1536]{2,1,0:T(8,128)(2,1)S(1)} %copy-done.3), custom_call_target="tpu_custom_call" | custom-call | tf_op jit(solution)/shard_map/pallas_call | solution.py:28
  77.6 2.6 %all-to-all-start.3 = ((bf16[32,40,128]{2,1,0:T(8,128)(2,1)}), bf16[32,40,128]{2,1,0:T(8,128)(2,1)S(1)}, u32[]{:S(2)}, u32[]{:S(2)}) async-start(bf16[32,40,128]{2,1,0:T(8,128)(2,1)} %shard_map.173), calls=%async_computation.3 | async-start | bytes 655360 | tf_op jit(solution)/shard_map/all_to_all | solution.py:436
  80.2 0.0 copy-done.6
  80.2 0.0 copy-start.8
  80.2 0.8 copy-done.8
  81.0 0.0 copy-start.12
  81.0 5.3 %shard_map.175 = bf16[15,6,128,128]{3,2,1,0:T(8,128)(2,1)} custom-call(f32[16,768]{1,0:T(8,128)S(1)} %copy-done.6, f32[16,768]{1,0:T(8,128)S(1)} %copy-done.8, bf16[15,6,128,128]{3,2,1,0:T(8,128)(2,1)S(1)} %copy-done), custom_call_target="tpu_custom_call" | custom-call | flops 10000000 | bytes 5898240 | tf_op jit(solution)/shard_map/pallas_call | solution.py:28
  86.3 5.6 %all-to-all-done.3.back_ref = bf16[32,40,128]{2,1,0:T(8,128)(2,1)S(1)} async-done(((bf16[32,40,128]{2,1,0:T(8,128)(2,1)}), bf16[32,40,128]{2,1,0:T(8,128)(2,1)S(1)}, u32[]{:S(2)}, u32[]{:S(2)}) %all-to-all-start.3) | async-done | bytes 327712 | tf_op jit(solution)/shard_map/all_to_all | solution.py:436
  91.9 0.0 copy-done.12
  91.9 1.0 %shard_map.174 = bf16[15,768]{1,0:T(8,128)(2,1)} custom-call(bf16[32,40,128]{2,1,0:T(8,128)(2,1)S(1)} %all-to-all-done.3.back_ref, s32[6,15]{1,0:T(8,128)S(1)} %bitcast.15, f32[6,15]{1,0:T(8,128)S(1)} %bitcast.16, f32[15,768]{1,0:T(8,128)S(1)} %get-tuple-element.19.own_ref), custom_call_target="tpu_custom_call" | custom-call | tf_op jit(solution)/shard_map/pallas_call | solution.py:28
  (1 shorter events, 0.0 us)
Async XLA Ops:
  0.6 46.7 %copy-start = (bf16[15,6,128,128]{3,2,1,0:T(8,128)(2,1)S(1)}, bf16[15,6,128,128]{3,2,1,0:T(8,128)(2,1)}, u32[]{:S(2)}) copy-start(bf16[15,6,128,128]{3,2,1,0:T(8,128)(2,1)} %state_ref.3) | copy-start | bytes 8847364
  0.6 46.7 %copy-start.11 = (f32[768]{0:T(1024)S(1)}, f32[768]{0:T(1024)}, u32[]{:S(2)}) copy-start(f32[768]{0:T(1024)} %lower_ref.1) | copy-start | bytes 9220
  2.8 15.8 %collective-permute-start = (bf16[4,96,768]{2,1,0:T(8,128)(2,1)S(1)}, bf16[4,96,768]{2,1,0:T(8,128)(2,1)S(1)}, u32[]{:S(2)}, u32[]{:S(2)}) collective-permute-start(bf16[4,96,768]{2,1,0:T(8,128)(2,1)S(1)} %get-tuple-element.13.own_ref), channel_id=1, source_target_pairs={{0,2},{2,0},{1,3},{3,1},{4,6},{6,4},{5,7},{7,5},{8,10},{10,8},{9,1... | collective-permute-start | bytes 1769480 | tf_op jit(solution)/shard_map/ppermute | solution.py:329
  19.7 42.1 %copy-start.4 = (bf16[15,1536]{1,0:T(8,128)(2,1)S(1)}, bf16[15,1536]{1,0:T(8,128)(2,1)}, u32[]{:S(2)}) copy-start(bf16[15,1536]{1,0:T(8,128)(2,1)} %refs_4_.1) | copy-start | bytes 138244
  19.7 42.1 %copy-start.9 = (s32[15,6]{0,1:T(8,128)S(1)}, s32[15,6]{0,1:T(8,128)}, u32[]{:S(2)}) copy-start(s32[15,6]{0,1:T(8,128)} %param.27) | copy-start | bytes 1084
  19.7 42.1 %copy-start.10 = (f32[1536]{0:T(1024)S(1)}, f32[1536]{0:T(1024)}, u32[]{:S(2)}) copy-start(f32[1536]{0:T(1024)} %refs_5_.1) | copy-start | bytes 18436
  19.8 27.6 %all-to-all-start.1 = ((bf16[16,16,768]{2,1,0:T(8,128)(2,1)}), bf16[16,16,768]{2,1,0:T(8,128)(2,1)S(1)}, u32[]{:S(2)}, u32[]{:S(2)}) async-start(bf16[16,16,768]{2,1,0:T(8,128)(2,1)} %bitcast.5), calls=%async_computation.1 | async-start | bytes 786432 | tf_op jit(solution)/shard_map/all_to_all | solution.py:350
  24.1 18.0 %collective-permute-start.2 = (bf16[96,768]{1,0:T(8,128)(2,1)}, bf16[96,768]{1,0:T(8,128)(2,1)S(1)}, u32[]{:S(2)}, u32[]{:S(2)}) collective-permute-start(bf16[96,768]{1,0:T(8,128)(2,1)} %get-tuple-element.15.own_ref), channel_id=1, source_target_pairs={{0,16},{8,24},{16,0},{24,8},{1,17},{9,25},{17,1},{25,9},{2,18},{10... | collective-permute-start | bytes 442376 | tf_op jit(solution)/shard_map/ppermute | solution.py:331
  26.9 16.8 %collective-permute-start.4 = (bf16[96,768]{1,0:T(8,128)(2,1)}, bf16[96,768]{1,0:T(8,128)(2,1)S(1)}, u32[]{:S(2)}, u32[]{:S(2)}) collective-permute-start(bf16[96,768]{1,0:T(8,128)(2,1)} %get-tuple-element.15.own_ref), channel_id=1, source_target_pairs={{0,8},{8,0},{16,24},{24,16},{1,9},{9,1},{17,25},{25,17},{2,10},{10... | collective-permute-start | bytes 442376 | tf_op jit(solution)/shard_map/ppermute | solution.py:332
  42.1 5.2 %collective-permute-start.6 = (bf16[96,768]{1,0:T(8,128)(2,1)S(1)}, bf16[96,768]{1,0:T(8,128)(2,1)}, u32[]{:S(2)}, u32[]{:S(2)}) collective-permute-start(bf16[96,768]{1,0:T(8,128)(2,1)S(1)} %collective-permute-done.2.far_ref), channel_id=1, source_target_pairs={{0,8},{8,0},{16,24},{24,16},{1,9},{9,1},{17,25},{25,17},{2,10},{10... | collective-permute-start | bytes 442376 | tf_op jit(solution)/shard_map/ppermute | solution.py:344
  43.7 7.0 %collective-permute-start.3 = (bf16[2,96,768]{2,1,0:T(8,128)(2,1)}, bf16[2,96,768]{2,1,0:T(8,128)(2,1)}, u32[]{:S(2)}, u32[]{:S(2)}) collective-permute-start(bf16[2,96,768]{2,1,0:T(8,128)(2,1)} %shard_map.170.refs_2_), channel_id=1, source_target_pairs={{0,2},{2,0},{1,3},{3,1},{4,6},{6,4},{5,7},{7,5},{8,10},{10,8},{9,1... | collective-permute-start | bytes 884744 | tf_op jit(solution)/shard_map/ppermute | solution.py:345
  43.8 7.0 %collective-permute-start.5 = (bf16[96,768]{1,0:T(8,128)(2,1)S(1)}, bf16[96,768]{1,0:T(8,128)(2,1)}, u32[]{:S(2)}, u32[]{:S(2)}) collective-permute-start(bf16[96,768]{1,0:T(8,128)(2,1)S(1)} %collective-permute-done.4.refs_4_), channel_id=1, source_target_pairs={{0,2},{2,0},{1,3},{3,1},{4,6},{6,4},{5,7},{7,5},{8,10},{10,8},{9,1... | collective-permute-start | bytes 442376 | tf_op jit(solution)/shard_map/ppermute | solution.py:346
  47.3 3.4 %collective-permute-start.7 = (bf16[96,768]{1,0:T(8,128)(2,1)}, bf16[96,768]{1,0:T(8,128)(2,1)}, u32[]{:S(2)}, u32[]{:S(2)}) collective-permute-start(bf16[96,768]{1,0:T(8,128)(2,1)} %collective-permute-done.6.refs_6_), channel_id=1, source_target_pairs={{0,2},{2,0},{1,3},{3,1},{4,6},{6,4},{5,7},{7,5},{8,10},{10,8},{9,1... | collective-permute-start | bytes 442376 | tf_op jit(solution)/shard_map/ppermute | solution.py:347
  47.3 28.8 %copy-start.1 = (bf16[1,1536,256]{2,1,0:T(8,128)(2,1)S(1)}, bf16[1,1536,256]{2,1,0:T(8,128)(2,1)}, u32[]{:S(2)}) copy-start(bf16[1,1536,256]{2,1,0:T(8,128)(2,1)} %gate_ref.1) | copy-start | bytes 2359300
  47.3 28.8 %copy-start.2 = (bf16[1,1536,256]{2,1,0:T(8,128)(2,1)S(1)}, bf16[1,1536,256]{2,1,0:T(8,128)(2,1)}, u32[]{:S(2)}) copy-start(bf16[1,1536,256]{2,1,0:T(8,128)(2,1)} %up_ref.1) | copy-start | bytes 2359300
  47.4 28.8 %copy-start.3 = (bf16[1,256,1536]{2,1,0:T(8,128)(2,1)S(1)}, bf16[1,256,1536]{2,1,0:T(8,128)(2,1)}, u32[]{:S(2)}) copy-start(bf16[1,256,1536]{2,1,0:T(8,128)(2,1)} %down_ref.1) | copy-start | bytes 2359300
  47.4 0.8 copy-start.13
  49.3 26.8 %copy-start.5 = (f32[16,768]{1,0:T(8,128)}, f32[16,768]{1,0:T(8,128)S(1)}, u32[]{:S(2)}) copy-start(f32[16,768]{1,0:T(8,128)S(1)} %get-tuple-element.20.forget_ref) | copy-start | bytes 147460
  49.3 26.8 %copy-start.7 = (f32[16,768]{1,0:T(8,128)}, f32[16,768]{1,0:T(8,128)S(1)}, u32[]{:S(2)}) copy-start(f32[16,768]{1,0:T(8,128)S(1)} %get-tuple-element.21.value_ref) | copy-start | bytes 147460
  49.3 3.9 %collective-permute-start.1 = (bf16[16,768]{1,0:T(8,128)(2,1)S(1)}, bf16[16,768]{1,0:T(8,128)(2,1)S(1)}, u32[]{:S(2)}, u32[]{:S(2)}) collective-permute-start(bf16[16,768]{1,0:T(8,128)(2,1)S(1)} %get-tuple-element.14.refs_0_), channel_id=1, source_target_pairs={{0,4},{4,0},{1,5},{5,1},{2,6},{6,2},{3,7},{7,3},{8,12},{12,8},{9,1... | collective-permute-start | bytes 73736 | tf_op jit(solution)/shard_map/ppermute | solution.py:367
  55.0 3.9 %collective-permute-start.8 = (bf16[16,768]{1,0:T(8,128)(2,1)S(1)}, bf16[16,768]{1,0:T(8,128)(2,1)S(1)}, u32[]{:S(2)}, u32[]{:S(2)}) collective-permute-start(bf16[16,768]{1,0:T(8,128)(2,1)S(1)} %get-tuple-element.16.refs_0_), channel_id=1, source_target_pairs={{0,1},{1,0},{4,5},{5,4},{2,3},{3,2},{6,7},{7,6},{8,9},{9,8},{12,13... | collective-permute-start | bytes 73736 | tf_op jit(solution)/shard_map/ppermute | solution.py:401
  56.6 4.7 %collective-permute-start.10 = (bf16[16,768]{1,0:T(8,128)(2,1)S(1)}, bf16[16,768]{1,0:T(8,128)(2,1)S(1)}, u32[]{:S(2)}, u32[]{:S(2)}) collective-permute-start(bf16[16,768]{1,0:T(8,128)(2,1)S(1)} %get-tuple-element.17), channel_id=1, source_target_pairs={{0,5},{1,4},{4,1},{5,0},{2,7},{3,6},{6,3},{7,2},{8,13},{9,12},{12,... | collective-permute-start | bytes 73736 | tf_op jit(solution)/shard_map/ppermute | solution.py:401
  58.0 3.8 %collective-permute-start.9 = (bf16[16,768]{1,0:T(8,128)(2,1)S(1)}, bf16[16,768]{1,0:T(8,128)(2,1)S(1)}, u32[]{:S(2)}, u32[]{:S(2)}) collective-permute-start(bf16[16,768]{1,0:T(8,128)(2,1)S(1)} %get-tuple-element.17), channel_id=1, source_target_pairs={{0,4},{1,5},{4,0},{5,1},{2,6},{3,7},{6,2},{7,3},{8,12},{9,13},{12,... | collective-permute-start | bytes 73736 | tf_op jit(solution)/shard_map/ppermute | solution.py:401
  76.1 4.0 %copy-start.6 = (f32[16,768]{1,0:T(8,128)S(1)}, f32[16,768]{1,0:T(8,128)}, u32[]{:S(2)}) copy-start(f32[16,768]{1,0:T(8,128)} %copy-done.5) | copy-start | bytes 147460
  77.6 14.3 %all-to-all-start.3 = ((bf16[32,40,128]{2,1,0:T(8,128)(2,1)}), bf16[32,40,128]{2,1,0:T(8,128)(2,1)S(1)}, u32[]{:S(2)}, u32[]{:S(2)}) async-start(bf16[32,40,128]{2,1,0:T(8,128)(2,1)} %shard_map.173), calls=%async_computation.3 | async-start | bytes 655360 | tf_op jit(solution)/shard_map/all_to_all | solution.py:436
  80.2 0.8 copy-start.8
  81.0 10.9 %copy-start.12 = (f32[15,6]{0,1:T(8,128)S(1)}, f32[15,6]{0,1:T(8,128)}, u32[]{:S(2)}) copy-start(f32[15,6]{0,1:T(8,128)} %param.28) | copy-start | bytes 1084
